TPU v7x, 256 devices: a 4x2x16 block of a 4x16x16 slice. The times are simulated.
256 devices in a mesh: grp: 2 (over y), sp: 32 (over z, core), tp: 4 (over x).
Axes of the slice: x: 4, y: 2, z: 16, core: 2. Of those that a mesh axis runs over, the one named last changes fastest.
The devices are a block of a 4x16x16 slice.
Arguments:
- residual: bfloat16 [49152, 2048], P(('grp', 'sp', 'tp')), parts along dimension 0, may hold values from -6 to 6
- value_projected: bfloat16 [49152, 4096], P(('grp', 'sp'), 'tp'), parts along dimension 0, may hold values from -6 to 6
- gate_projected: bfloat16 [49152, 4096], P(('grp', 'sp'), 'tp'), parts along dimension 0, may hold values from -6 to 6
- wide_key_rows: bfloat16 [49152, 1024], P(('grp', 'sp'), 'tp'), parts along dimension 0, may hold values from -6 to 6
- wide_query_rows: bfloat16 [49152, 1024], P(('grp', 'sp'), 'tp'), parts along dimension 0, may hold values from -6 to 6
- narrow_key_rows: bfloat16 [49152, 512], P(('grp', 'sp'), 'tp'), parts along dimension 0, may hold values from -6 to 6
- narrow_query_rows: bfloat16 [49152, 512], P(('grp', 'sp'), 'tp'), parts along dimension 0, may hold values from -6 to 6
- step_before_softplus: float32 [49152, 64], P(('grp', 'sp'), 'tp'), parts along dimension 0, may hold values from -5 to 5
- extra_log_decay: float32 [49152, 64], P(('grp', 'sp'), 'tp'), parts along dimension 0, may hold values from -0.7 to 0
- log_decay_rate: float32 [64], P('tp'), may hold values from -12.3 to -2.99
- value_kernel: bfloat16 [4, 4096], P(None, 'tp'), may hold values from -3 to 3
- wide_key_kernel: bfloat16 [4, 1024], P(None, 'tp'), may hold values from -3 to 3
- wide_query_kernel: bfloat16 [4, 1024], P(None, 'tp'), may hold values from -3 to 3
- narrow_key_kernel: bfloat16 [4, 512], P(None, 'tp'), may hold values from -3 to 3
- narrow_query_kernel: bfloat16 [4, 512], P(None, 'tp'), may hold values from -3 to 3
- head_norm_gain: bfloat16 [4096], P('tp'), may hold values from 0.099609375 to 1.8984375
- output_matrix: bfloat16 [4096, 2048], P('tp'), may hold values from -0.09375 to 0.09375
- feedforward_norm_gain: bfloat16 [2048], replicated, may hold values from 0.099609375 to 1.8984375
- gate_matrix: bfloat16 [2048, 3072], P('sp', 'tp'), may hold values from -0.125 to 0.125
- up_matrix: bfloat16 [2048, 3072], P('sp', 'tp'), may hold values from -0.125 to 0.125
- down_matrix: bfloat16 [2048, 3072], P('sp', 'tp'), may hold values from -0.3125 to 0.3125
Outputs:
- mixed: bfloat16 [49152, 2048], P(('grp', 'sp', 'tp')), parts along dimension 0
There are 2 independent parts, one for each index of `grp`. A program takes and returns all parts, laid end to end along the dimension named above; an argument that names none is the same for every part. Nothing has to cross between parts.
All inputs are finite; a program needn't handle non-finite values.
Results may differ from a plain program's by a relative error of at most 0.015.
Values may be sent and summed in bfloat16 or wider, within the bound.
A program may use at most 128 MiB of HBM per device.

v0:
```python
import functools
import jax
import jax.numpy as jnp
from jax import lax
from jax.experimental import pallas as pl
from jax.experimental.pallas import tpu as pltpu
from jax.sharding import PartitionSpec as P

F32 = jnp.float32
BF16 = jnp.bfloat16
MESH = pl.DeviceIdType.MESH
CH = 128
PAD = 16
GROUP_Q = (0, 256, 128, 384)
GROUP_K = (0, 256, 128, 256)
ROW_GROUP = ((0, 128, 0), (128, 256, 2), (256, 320, 1), (320, 384, 3))
HIGH = lax.Precision.HIGHEST


def pair_lanes(columns, head):
    rows = columns.shape[0]
    lane = lax.broadcasted_iota(jnp.int32, (rows, 128), 1)
    return jnp.where(
        lane < 64,
        jnp.broadcast_to(columns[:, head : head + 1], (rows, 128)),
        jnp.broadcast_to(columns[:, head + 1 : head + 2], (rows, 128)),
    )


def quad_lanes(columns, group):
    return jnp.concatenate(
        [pair_lanes(columns, 4 * group), pair_lanes(columns, 4 * group + 2)], axis=1
    )


def silu(x):
    return x / (1.0 + jnp.exp(-x))


def matmul(a, b, dims=((1,), (0,)), precision=None):
    return lax.dot_general(a, b, (dims, ((), ())), preferred_element_type=F32, precision=precision)


def group_of_row(row):
    for low, high, group in ROW_GROUP:
        if low <= row < high:
            return group


def mixer_kernel(
    peers,
    value_ref,
    wk_ref,
    wq_ref,
    nk_ref,
    nq_ref,
    gate_ref,
    step_ref,
    extra_ref,
    rate_ref,
    vker_ref,
    wkker_ref,
    wqker_ref,
    nkker_ref,
    nqker_ref,
    gain_ref,
    normed_ref,
    xpad,
    ubuf,
    kbuf,
    qbuf,
    gbuf,
    rcol,
    qrow,
    total,
    ebuf,
    hbuf,
    ybuf,
    out_msg,
    in_msg,
    out_ret,
    in_ret,
    hent,
    local_sem,
    rim_send,
    rim_recv,
    send_a,
    recv_a,
    send_b,
    recv_b,
):
    length = value_ref.shape[0]
    count = length // CH
    me = lax.axis_index("sp")
    inputs = (value_ref, wk_ref, wq_ref, nk_ref, nq_ref)
    spans = []
    at = 0
    for ref in inputs:
        spans.append((at, at + ref.shape[1]))
        at += ref.shape[1]
    loads = [
        pltpu.make_async_copy(
            ref, xpad.at[pl.ds(PAD, length), pl.ds(low, high - low)], local_sem.at[n]
        )
        for n, (ref, (low, high)) in enumerate(zip(inputs, spans))
    ]
    loads.append(pltpu.make_async_copy(gate_ref, gbuf, local_sem.at[len(inputs)]))
    for load in loads:
        load.start()
    rims = []
    if peers > 1:
        barrier = pltpu.get_barrier_semaphore()
        for offset in range(1, peers):
            pl.semaphore_signal(
                barrier,
                inc=1,
                device_id={"sp": lax.rem(me + offset, peers)},
                device_id_type=MESH,
            )
        pl.semaphore_wait(barrier, peers - 1)
        for n, (ref, (low, high)) in enumerate(zip(inputs, spans)):
            rims.append(
                pltpu.make_async_remote_copy(
                    src_ref=ref.at[pl.ds(length - PAD, PAD)],
                    dst_ref=xpad.at[pl.ds(0, PAD), pl.ds(low, high - low)],
                    send_sem=rim_send.at[n],
                    recv_sem=rim_recv.at[n],
                    device_id={"sp": lax.rem(me + 1, peers)},
                    device_id_type=MESH,
                )
            )
        for rim in rims:
            rim.start()
    for load in loads[:-1]:
        load.wait()

    row_id = lax.broadcasted_iota(jnp.int32, (CH, CH), 0)
    col_id = lax.broadcasted_iota(jnp.int32, (CH, CH), 1)
    lower = row_id >= col_id
    tril = lower.astype(F32)
    triu = (row_id <= col_id).astype(F32)
    eye = (row_id == col_id).astype(F32)
    left = lax.broadcasted_iota(jnp.int32, (CH, 128), 1) < 64
    kernels = (vker_ref, wkker_ref, wqker_ref, nkker_ref, nqker_ref)

    def conv_tile(base, which, tile):
        low = spans[which][0] + 128 * tile
        columns = pl.ds(low, 128)
        before = xpad[pl.ds(base, PAD), columns].astype(F32)[PAD - 8 :]
        here = xpad[pl.ds(base + PAD, CH), columns].astype(F32)
        rows = jnp.concatenate([before, here], axis=0)
        taps = kernels[which][:, 128 * tile : 128 * tile + 128].astype(F32)
        acc = here * taps[3:4]
        for tap in range(3):
            acc = acc + pltpu.roll(rows, 3 - tap, 0)[8:] * taps[tap : tap + 1]
        return silu(acc)

    def first_pass(i, carry):
        c = lax.rem(i + 1, count)
        base = pl.multiple_of(c * CH, CH)

        @pl.when(i == count - 1)
        def _():
            for rim in rims:
                rim.wait()

            @pl.when(me == 0)
            def _():
                xpad[0:PAD, :] = jnp.zeros((PAD, xpad.shape[1]), BF16)

        here = pl.ds(base, CH)
        dt = step_ref[here, :]
        dt = jnp.maximum(dt, 0.0) + jnp.log(1.0 + jnp.exp(-jnp.abs(dt)))
        a = -jnp.exp(rate_ref[...]) * dt + extra_ref[here, :]
        r = matmul(tril, a, precision=HIGH)
        r_row = matmul(a, triu, ((0,), (0,)), HIGH)
        dt_row = matmul(dt, eye, ((0,), (0,)), HIGH)
        rcol[here, :] = r
        qrow[c] = r_row - jnp.log(dt_row)
        end = r[CH - 1 : CH, :]
        total[c] = end
        fade = dt * jnp.exp(end - r)
        for tile in range(2):
            kbuf[here, 128 * tile : 128 * tile + 128] = conv_tile(base, 1, tile).astype(BF16)
            qbuf[here, 128 * tile : 128 * tile + 128] = conv_tile(base, 2, tile).astype(BF16)
        kbuf[here, 256:384] = conv_tile(base, 3, 0).astype(BF16)
        narrow_q = conv_tile(base, 4, 0)
        qbuf[here, 256:384] = jnp.where(left, narrow_q, 0.0).astype(BF16)
        qbuf[here, 384:512] = jnp.where(left, 0.0, narrow_q).astype(BF16)
        for group in range(4):
            parts = []
            for half in range(2):
                pair = 2 * group + half
                u = conv_tile(base, 0, pair).astype(BF16)
                ubuf[here, 128 * pair : 128 * pair + 128] = u
                parts.append((u.astype(F32) * pair_lanes(fade, 2 * pair)).astype(BF16))
            v = jnp.concatenate(parts, axis=1)
            k = kbuf[here, GROUP_K[group] : GROUP_K[group] + 128]
            e = matmul(k, v, ((0,), (0,)))
            if group == 0:
                ebuf[c, 0:128, :] = e
            elif group == 2:
                ebuf[c, 128:256, :] = e
            elif group == 1:
                ebuf[c, 256:320, :] = e[0:64]
            else:
                ebuf[c, 320:384, :] = e[64:128]
        return carry

    lax.fori_loop(0, count, first_pass, 0)

    offsets = [jnp.zeros((1, 16), F32)]
    for c in range(count):
        offsets.append(offsets[-1] + total[c])
    whole = offsets[-1]
    for low, high, group in ROW_GROUP:
        state = jnp.zeros((high - low, 256), F32)
        for c in range(count):
            hbuf[c, low:high, :] = state.astype(BF16)
            state = state * jnp.exp(quad_lanes(total[c], group)) + ebuf[c, low:high, :]
        hent[low:high, :] = state

    if peers > 1:
        per = 384 // (peers // 2)
        wide_log = [quad_lanes(whole, group) for group in range(4)]
        sub = lax.broadcasted_iota(jnp.int32, (8, 128), 0)
        for slot in range(peers):
            z, core = slot // 2, slot % 2
            lanes = slice(128 * core, 128 * core + 128)
            logs = jnp.zeros((8, 128), F32)
            for tile in range(per // 8):
                line = wide_log[group_of_row(per * z + 8 * tile)][:, lanes]
                logs = jnp.where(sub == tile, jnp.broadcast_to(line, (8, 128)), logs)
            body = hent[per * z : per * z + per, lanes]
            out_msg[slot] = jnp.concatenate([body, logs], axis=0).astype(BF16)

        def exchange(source, target, send, recv):
            order = sorted(range(1, peers), key=lambda o: -min(o, peers - o))
            copies = []
            for offset in order:
                to = lax.rem(me + offset, peers)
                copies.append(
                    pltpu.make_async_remote_copy(
                        src_ref=source.at[to],
                        dst_ref=target.at[me],
                        send_sem=send.at[offset],
                        recv_sem=recv.at[offset],
                        device_id={"sp": to},
                        device_id_type=MESH,
                    )
                )
            return copies

        phase_a = exchange(out_msg, in_msg, send_a, recv_a)
        for copy in phase_a:
            copy.start()
        in_msg[me] = out_msg[me]

    for c in range(count):
        here = slice(c * CH, c * CH + CH)
        r = rcol[here, :]
        fade_out = jnp.exp(r)
        for group in range(4):
            q = qbuf[here, GROUP_Q[group] : GROUP_Q[group] + 128]
            k = kbuf[here, GROUP_K[group] : GROUP_K[group] + 128]
            score = matmul(q, k, ((1,), (1,)))
            row = 0 if group == 0 else 128 if group == 2 else 256
            outer = matmul(q, hbuf[c, row : row + 128, :])
            for half in range(2):
                pair = 2 * group + half
                weights = []
                for head in (2 * pair, 2 * pair + 1):
                    gap = jnp.broadcast_to(r[:, head : head + 1], (CH, CH)) - qrow[c, head : head + 1, :]
                    w = score * jnp.exp(jnp.where(lower, gap, -jnp.inf))
                    weights.append(w.astype(BF16))
                u = ubuf[here, 128 * pair : 128 * pair + 128].astype(F32)
                both = jnp.concatenate(
                    [jnp.where(left, u, 0.0).astype(BF16), jnp.where(left, 0.0, u).astype(BF16)],
                    axis=0,
                )
                inner = matmul(jnp.concatenate(weights, axis=1), both)
                ybuf[here, 128 * pair : 128 * pair + 128] = (
                    inner + outer[:, 128 * half : 128 * half + 128] * pair_lanes(fade_out, 2 * pair)
                )

    if peers > 1:
        for copy in phase_a:
            copy.wait()
        tiles = per // 8
        state = [jnp.zeros((8, 128), F32) for _ in range(tiles)]
        for source in range(peers):
            out_ret[source] = jnp.concatenate(
                state + [jnp.zeros((8, 128), F32)], axis=0
            ).astype(BF16)
            message = in_msg[source].astype(F32)
            for tile in range(tiles):
                decay = jnp.exp(message[per + tile : per + tile + 1, :])
                state[tile] = state[tile] * decay + message[8 * tile : 8 * tile + 8, :]
        phase_b = exchange(out_ret, in_ret, send_b, recv_b)
        for copy in phase_b:
            copy.start()
        in_ret[me] = out_ret[me]

    loads[-1].wait()
    if peers > 1:
        for copy in phase_b:
            copy.wait()
        for slot in range(peers):
            z, core = slot // 2, slot % 2
            hent[per * z : per * z + per, 128 * core : 128 * core + 128] = in_ret[slot].astype(
                F32
            )[:per]
    ones = (
        (row_id < 64) == (col_id < 64)
    ).astype(BF16)

    for c in range(count):
        here = slice(c * CH, c * CH + CH)
        reach = jnp.exp(rcol[here, :] + offsets[c])
        for group in range(4):
            if peers > 1:
                q = qbuf[here, GROUP_Q[group] : GROUP_Q[group] + 128]
                row = 0 if group == 0 else 128 if group == 2 else 256
                entered = matmul(q, hent[row : row + 128, :].astype(BF16))
            for half in range(2):
                pair = 2 * group + half
                lanes = slice(128 * pair, 128 * pair + 128)
                y = ybuf[here, lanes]
                if peers > 1:
                    y = y + entered[:, 128 * half : 128 * half + 128] * pair_lanes(reach, 2 * pair)
                gated = y * silu(gbuf[here, lanes].astype(F32))
                square = matmul((gated * gated).astype(BF16), ones)
                scale = lax.rsqrt(square * (1.0 / 64.0) + 1e-06)
                normed_ref[here, lanes] = (
                    gated * scale * gain_ref[:, lanes].astype(F32)
                ).astype(BF16)


def mixer(arrays, peers):
    length = arrays[0].shape[0]
    width = sum(a.shape[1] for a in arrays[:5])
    count = length // CH
    channels = arrays[0].shape[1]
    message = 384 // max(peers // 2, 1) + 8
    any_space = pl.BlockSpec(memory_space=pl.ANY)
    vmem = pl.BlockSpec(memory_space=pltpu.VMEM)
    dma = pltpu.SemaphoreType.DMA
    params = dict(vmem_limit_bytes=56 * 1024 * 1024)
    if peers > 1:
        params.update(collective_id=1, has_side_effects=True)
    return pl.pallas_call(
        functools.partial(mixer_kernel, peers),
        out_shape=jax.ShapeDtypeStruct((length, channels), BF16),
        in_specs=[any_space] * 6 + [vmem] * 9,
        out_specs=vmem,
        scratch_shapes=[
            pltpu.VMEM((PAD + length, width), BF16),
            pltpu.VMEM((length, channels), BF16),
            pltpu.VMEM((length, 384), BF16),
            pltpu.VMEM((length, 512), BF16),
            pltpu.VMEM((length, channels), BF16),
            pltpu.VMEM((length, 16), F32),
            pltpu.VMEM((count, 16, CH), F32),
            pltpu.VMEM((count, 1, 16), F32),
            pltpu.VMEM((count, 384, 256), F32),
            pltpu.VMEM((count, 384, 256), BF16),
            pltpu.VMEM((length, channels), F32),
            pltpu.VMEM((peers, message, 128), BF16),
            pltpu.VMEM((peers, message, 128), BF16),
            pltpu.VMEM((peers, message, 128), BF16),
            pltpu.VMEM((peers, message, 128), BF16),
            pltpu.VMEM((384, 256), F32),
            dma((6,)),
            dma((5,)),
            dma((5,)),
            dma((peers,)),
            dma((peers,)),
            dma((peers,)),
            dma((peers,)),
        ],
        compiler_params=pltpu.CompilerParams(**params),
        cost_estimate=pl.CostEstimate(
            flops=80_000_000_000, bytes_accessed=8_000_000, transcendentals=0
        ),
        name="mixer",
    )(*arrays)


def sent_together(arrays, axis, dim, along):
    ends, at = ([], 0)
    for a in arrays[:-1]:
        at += a.shape[along]
        ends.append(at)
    both = jnp.concatenate(arrays, axis=along)
    return tuple(jnp.split(lax.all_gather(both, axis, axis=dim, tiled=True), ends, axis=along))


def in_blocks(shard, dim, size):
    before, after = (shard.shape[:dim], shard.shape[dim + 1 :])
    return jnp.moveaxis(shard.reshape(*before, size, -1, *after), dim, 0)


def summed_on_arrival(shard, axis, dim):
    pieces = in_blocks(shard, dim, lax.axis_size(axis))
    arrived = lax.all_to_all(pieces, axis, split_axis=0, concat_axis=0, tiled=True)
    return arrived.astype(jnp.float32).sum(axis=0)


def on_device(
    residual,
    value_projected,
    gate_projected,
    wide_key_rows,
    wide_query_rows,
    narrow_key_rows,
    narrow_query_rows,
    step_before_softplus,
    extra_log_decay,
    log_decay_rate,
    value_kernel,
    wide_key_kernel,
    wide_query_kernel,
    narrow_key_kernel,
    narrow_query_kernel,
    head_norm_gain,
    output_matrix,
    feedforward_norm_gain,
    gate_matrix,
    up_matrix,
    down_matrix,
):
    normed = mixer(
        [
            value_projected,
            wide_key_rows,
            wide_query_rows,
            narrow_key_rows,
            narrow_query_rows,
            gate_projected,
            step_before_softplus,
            extra_log_decay,
            log_decay_rate[None],
            value_kernel,
            wide_key_kernel,
            wide_query_kernel,
            narrow_key_kernel,
            narrow_query_kernel,
            head_norm_gain[None],
        ],
        lax.axis_size("sp"),
    )
    projected = summed_on_arrival(
        jnp.dot(normed, output_matrix, preferred_element_type=jnp.float32).astype(jnp.bfloat16),
        "tp",
        0,
    )
    after_mixer = (residual.astype(jnp.float32) + projected).astype(jnp.bfloat16)
    rows = after_mixer.astype(jnp.float32)
    x_norm = (
        rows
        * lax.rsqrt(jnp.mean(rows * rows, axis=-1, keepdims=True) + 1e-06)
        * feedforward_norm_gain.astype(jnp.float32)
    ).astype(jnp.bfloat16)
    gate_full, up_full, down_full = sent_together((gate_matrix, up_matrix, down_matrix), "sp", 0, 1)
    x_norm, gate_full, up_full, down_full = lax.optimization_barrier(
        (x_norm, gate_full, up_full, down_full)
    )
    piece = lax.all_gather(x_norm, "tp", axis=0, tiled=True)
    gate_values = jnp.dot(piece, gate_full, preferred_element_type=jnp.float32)
    up_values = jnp.dot(piece, up_full, preferred_element_type=jnp.float32)
    hidden = (jax.nn.silu(gate_values) * up_values).astype(jnp.bfloat16)
    channel = summed_on_arrival(
        lax.dot_general(
            hidden, down_full, (((1,), (1,)), ((), ())), preferred_element_type=jnp.float32
        ).astype(jnp.bfloat16),
        "tp",
        0,
    )
    return (after_mixer.astype(jnp.float32) + 0.5 * channel).astype(jnp.bfloat16)


def solution(mesh):
    in_specs = (
        P(("grp", "sp", "tp"), None),
        P(("grp", "sp"), "tp"),
        P(("grp", "sp"), "tp"),
        P(("grp", "sp"), "tp"),
        P(("grp", "sp"), "tp"),
        P(("grp", "sp"), "tp"),
        P(("grp", "sp"), "tp"),
        P(("grp", "sp"), "tp"),
        P(("grp", "sp"), "tp"),
        P("tp"),
        P(None, "tp"),
        P(None, "tp"),
        P(None, "tp"),
        P(None, "tp"),
        P(None, "tp"),
        P("tp"),
        P("tp", None),
        P(),
        P("sp", "tp"),
        P("sp", "tp"),
        P("sp", "tp"),
    )
    out_specs = P(("grp", "sp", "tp"), None)
    return jax.shard_map(
        on_device, mesh=mesh, in_specs=in_specs, out_specs=out_specs, check_vma=False
    )
```

profile of v0, /device:TPU:33, one launch (start us, length us, event | category | flops | bytes accessed | tf_op | source)
XLA Modules:
  0.0 250.4 jit_solution(558722517182599979)
XLA Ops:
  6.5 0.0 all-gather.3.cloned.1.call-start
  6.6 1.7 pad_maximum_fusion
  8.3 0.1 all-gather.3.cloned.1.call-update
  8.3 1.3 broadcast_in_dim.9.gain_ref
  9.6 1.7 copy.22.step_ref
  11.3 1.7 copy.23.extra_ref
  13.0 0.0 copy-start.2
  13.0 71.6 %mixer.1 = bf16[768,1024]{1,0:T(8,128)(2,1)} custom-call(bf16[768,1024]{1,0:T(8,128)(2,1)} %value_ref.1, bf16[768,256]{1,0:T(8,128)(2,1)} %wk_ref.1, bf16[768,256]{1,0:T(8,128)(2,1)} %wq_ref.1, bf16[768,128]{1,0:T(8,128)(2,1)} %nk_ref.1, bf16[768,128]{1,0:T(8,128)(2,1)} %nq_ref.1, bf16[768,1024]{1,0:T(8,128)(2,1)} %gate_ref.1, f32[768,16]{1,0:T(8,128)} %copy.22.step_ref, ...), custom_call_target="tpu_custom_call" | custom-call | flops 80000000000 | bytes 8000000 | tf_op jit(solution)/shard_map/mixer/pallas_call | solution.py:351
  84.6 0.0 copy-done.2
  84.6 6.3 %convolution_convert_fusion.1 = bf16[768,2048]{1,0:T(8,128)(2,1)} fusion(bf16[768,1024]{1,0:T(8,128)(2,1)} %mixer.1, bf16[1024,2048]{1,0:T(8,128)(2,1)S(1)} %copy-done.2), kind=kOutput, calls=%fused_computation.3 | convolution fusion | flops 3222798336 | bytes 8912896 | tf_op jit(solution)/shard_map/dot_general | solution.py:453
  90.9 0.0 copy-start.1
  90.9 5.0 %all-to-all-start = ((bf16[4,192,2048]{2,1,0:T(8,128)(2,1)}), bf16[4,192,2048]{2,1,0:T(8,128)(2,1)S(1)}, u32[]{:S(2)}, u32[]{:S(2)}) async-start(bf16[4,192,2048]{2,1,0:T(8,128)(2,1)} %bitcast.10), calls=%async_computation | async-start | bytes 6291456 | tf_op jit(solution)/shard_map/all_to_all | solution.py:405
  96.0 0.0 all-gather.5.cloned.1.call-start
  96.0 0.0 copy-done.1
  96.0 37.2 %all-to-all-done = bf16[4,192,2048]{2,1,0:T(8,128)(2,1)S(1)} async-done(((bf16[4,192,2048]{2,1,0:T(8,128)(2,1)}), bf16[4,192,2048]{2,1,0:T(8,128)(2,1)S(1)}, u32[]{:S(2)}, u32[]{:S(2)}) %all-to-all-start) | async-done | bytes 3145760 | tf_op jit(solution)/shard_map/all_to_all | solution.py:405
  133.2 0.0 copy-start
  133.2 0.6 convert_reduce_fusion.1
  133.8 0.5 copy-done
  134.3 0.3 fusion
  134.6 1.1 fusion.2
  135.8 0.0 all-gather.3.cloned.1.call-done
  135.8 6.9 %fusion.5 = (bf16[2048,768]{1,0:T(8,128)(2,1)}, bf16[2048,768]{1,0:T(8,128)(2,1)}, bf16[2048,768]{1,0:T(8,128)(2,1)}) fusion(bf16[2048,2304]{1,0:T(8,128)(2,1)} %all-gather.3.cloned.1.call-done), kind=kLoop, calls=%fused_computation.16 | loop fusion | bytes 18874368 | tf_op jit(solution)/shard_map/split | solution.py:395
  142.6 0.1 all-gather.5.cloned.1.call-update
  142.7 42.2 %all-gather.5.cloned.1.call-done = bf16[768,2048]{1,0:T(8,128)(2,1)} async-done(((bf16[192,2048]{1,0:T(8,128)(2,1)}), bf16[768,2048]{1,0:T(8,128)(2,1)}) %all-gather.5.cloned.1.call-update) | async-done | bytes 3145744 | tf_op jit(solution)/shard_map/all_gather | solution.py:468
  184.9 5.4 %fusion.6 = f32[768,768]{1,0:T(8,128)S(1)} fusion(bf16[768,2048]{1,0:T(8,128)(2,1)} %all-gather.5.cloned.1.call-done, bf16[2048,768]{1,0:T(8,128)(2,1)} %get-tuple-element.10), kind=kOutput, calls=%fused_computation.17 | convolution fusion | flops 2415919104 | bytes 8650752 | tf_op jit(solution)/shard_map/dot_general | solution.py:469
  190.4 11.2 %convolution_convert_fusion = bf16[768,2048]{1,0:T(8,128)(2,1)} fusion(bf16[2048,768]{1,0:T(8,128)(2,1)} %get-tuple-element.12, f32[768,768]{1,0:T(8,128)S(1)} %fusion.6, bf16[768,2048]{1,0:T(8,128)(2,1)} %all-gather.5.cloned.1.call-done, bf16[2048,768]{1,0:T(8,128)(2,1)} %get-tuple-element.11), kind=kOutput, calls=%fused_computation.2 | convolution fusion | flops 4836950016 | bytes 14942208 | tf_op jit(solution)/shard_map/dot_general | solution.py:473
  201.6 40.3 %all_to_all.10 = bf16[4,192,2048]{2,1,0:T(8,128)(2,1)S(1)} all-to-all(bf16[4,192,2048]{2,1,0:T(8,128)(2,1)} %bitcast.11), channel_id=1, replica_groups=mesh['grp'=2,'sp'=32,'tp'=4] {'tp'}, dimensions={0} | all-to-all | bytes 6291456 | tf_op jit(solution)/shard_map/all_to_all | solution.py:405
  241.9 0.6 convert_reduce_fusion
  242.5 1.1 fusion.3
  (2 shorter events, 0.0 us)
Async XLA Ops:
  6.5 129.2 %all-gather.3.cloned.1.call-start = ((), (), s32[]{:S(2)}) async-start(), calls=%async_computation.2 | async-start | bytes 9732096 | tf_op jit(solution)/shard_map/all_gather | solution.py:395
  13.0 71.6 %copy-start.2 = (bf16[1024,2048]{1,0:T(8,128)(2,1)S(1)}, bf16[1024,2048]{1,0:T(8,128)(2,1)}, u32[]{:S(2)}) copy-start(bf16[1024,2048]{1,0:T(8,128)(2,1)} %param.37) | copy-start | bytes 12582916
  90.9 5.1 %copy-start.1 = (bf16[2048]{0:T(1024)(128)(2,1)S(1)}, bf16[2048]{0:T(1024)(128)(2,1)}, u32[]{:S(2)}) copy-start(bf16[2048]{0:T(1024)(128)(2,1)} %param.38) | copy-start | bytes 12292
  90.9 42.3 %all-to-all-start = ((bf16[4,192,2048]{2,1,0:T(8,128)(2,1)}), bf16[4,192,2048]{2,1,0:T(8,128)(2,1)S(1)}, u32[]{:S(2)}, u32[]{:S(2)}) async-start(bf16[4,192,2048]{2,1,0:T(8,128)(2,1)} %bitcast.10), calls=%async_computation | async-start | bytes 6291456 | tf_op jit(solution)/shard_map/all_to_all | solution.py:405
  96.0 89.0 %all-gather.5.cloned.1.call-start = ((), (), s32[]{:S(2)}) async-start(), calls=%async_computation.3 | async-start | bytes 3932160 | tf_op jit(solution)/shard_map/all_gather | solution.py:468
  133.2 1.1 copy-start
Sparse Core Ops, SparseCore 0:
  9.2 114.2 all-gather.2
  142.8 42.0 all-gather.4
where the time goes:
time: 251 us; the launch traced here: 250 us
  waiting for transfers between devices  79.5 us (32%)
  Pallas kernels  71.6 us (29%)
  blocking collectives  40.3 us (16%)
  matrix products  22.9 us (9%)
  between operations  13.5 us (5%)
  local copies, waits for them, and re-layouts  12.1 us (5%)
  other arithmetic  5.48 us (2%)
  starting transfers between devices  5.05 us (2%)
    pallas_call x1, Pallas kernels, mixer(): pl.pallas_call(functools.partial(mixer_kernel, peers), out_shape=jax.Shap...  71.6 us
    all_gather x1, waiting for transfers between devices, on_device(): piece = lax.all_gather(x_norm, 'tp', axis=0, tiled=True)  42.2 us
    all_to_all x1, blocking collectives, summed_on_arrival(): lax.all_to_all(pieces, axis, split_axis=0, concat_axis=0, tiled=True)  40.3 us
    all_to_all x1, waiting for transfers between devices, summed_on_arrival(): lax.all_to_all(pieces, axis, split_axis=0, concat_axis=0, tiled=True)  37.2 us
    dot_general x1, matrix products, on_device(): lax.dot_general(hidden, down_full, (((1,), (1,)), ((), ())), preferred_el...  11.2 us
    split x1, local copies, waits for them, and re-layouts, sent_together(): jnp.split(lax.all_gather(both, axis, axis=dim, tiled=True), ends, axis=al...  6.85 us
    dot_general x1, matrix products, on_device(): jnp.dot(normed, output_matrix, preferred_element_type=jnp.float32)  6.27 us
    dot_general x1, matrix products, on_device(): gate_values = jnp.dot(piece, gate_full, preferred_element_type=jnp.float32)  5.44 us
  transfers between devices with their start and end apart: 3, of which 2 were waited for; matrix products, arithmetic and copies ran while one was open for 5% of the time, Pallas kernels for 29%

commit v1 on v0

--- a/solution.py
+++ b/solution.py
@@ -386,24 +386,340 @@
     )(*arrays)
 
 
-def sent_together(arrays, axis, dim, along):
-    ends, at = ([], 0)
-    for a in arrays[:-1]:
-        at += a.shape[along]
-        ends.append(at)
-    both = jnp.concatenate(arrays, axis=along)
-    return tuple(jnp.split(lax.all_gather(both, axis, axis=dim, tiled=True), ends, axis=along))
-
-
-def in_blocks(shard, dim, size):
-    before, after = (shard.shape[:dim], shard.shape[dim + 1 :])
-    return jnp.moveaxis(shard.reshape(*before, size, -1, *after), dim, 0)
-
-
-def summed_on_arrival(shard, axis, dim):
-    pieces = in_blocks(shard, dim, lax.axis_size(axis))
-    arrived = lax.all_to_all(pieces, axis, split_axis=0, concat_axis=0, tiled=True)
-    return arrived.astype(jnp.float32).sum(axis=0)
+ROW_PARTS = 2
+
+
+def silu_gate(x):
+    return x / (1.0 + jnp.exp(-x))
+
+
+class Reducer:
+    def __init__(self, axis, buffers, send, recv):
+        self.me = lax.axis_index(axis)
+        self.right = lax.rem(self.me + 1, 4)
+        self.left = lax.rem(self.me + 3, 4)
+        self.far = lax.rem(self.me + 2, 4)
+        self.axis = axis
+        (self.blocks, self.own, self.relay_r, self.relay_l, self.comb_r, self.comb_l,
+         self.from_l, self.from_r) = buffers
+        self.send, self.recv = send, recv
+        self.rows = self.own.shape[0] // ROW_PARTS
+        self.half = self.own.shape[1] // 2
+
+    def copy(self, part, index, source, target, to):
+        return pltpu.make_async_remote_copy(
+            src_ref=source,
+            dst_ref=target,
+            send_sem=self.send.at[part, index],
+            recv_sem=self.recv.at[part, index],
+            device_id={self.axis: to},
+            device_id_type=MESH,
+        )
+
+    def leg(self, part, index):
+        rows = pl.ds(part * self.rows, self.rows)
+        a, b = pl.ds(0, self.half), pl.ds(self.half, self.half)
+        source, target = (
+            (self.blocks.at[0, rows, a], self.relay_r.at[rows]),
+            (self.blocks.at[1, rows, b], self.from_l.at[rows, b]),
+            (self.comb_r.at[rows], self.from_l.at[rows, a]),
+            (self.blocks.at[0, rows, b], self.relay_l.at[rows]),
+            (self.blocks.at[2, rows, a], self.from_r.at[rows, a]),
+            (self.comb_l.at[rows], self.from_r.at[rows, b]),
+        )[index]
+        return self.copy(part, index, source, target, self.right if index < 3 else self.left)
+
+    def combine(self, part):
+        step = 32
+
+        for n, block, low, relay, comb in (
+            (0, 1, 0, self.relay_r, self.comb_r),
+            (3, 2, self.half, self.relay_l, self.comb_l),
+        ):
+            self.leg(part, n).wait_recv()
+
+            def body(i, carry, block=block, low=low, relay=relay, comb=comb):
+                rows = pl.ds(pl.multiple_of(part * self.rows + i * step, 16), step)
+                comb[rows, :] = (
+                    self.blocks[block, rows, low : low + self.half].astype(F32)
+                    + relay[rows, :].astype(F32)
+                ).astype(BF16)
+                return carry
+
+            lax.fori_loop(0, self.rows // step, body, 0)
+            self.leg(part, n + 2).start()
+
+    def wait_final(self, part):
+        for n in (1, 2, 4, 5):
+            self.leg(part, n).wait_recv()
+
+    def wait_sends(self):
+        for part in range(ROW_PARTS):
+            for n in range(6):
+                self.leg(part, n).wait_send()
+
+    def total(self, rows):
+        return (
+            self.own[rows, :]
+            + self.from_l[rows, :].astype(F32)
+            + self.from_r[rows, :].astype(F32)
+        )
+
+
+def greet(axis, others):
+    barrier = pltpu.get_barrier_semaphore()
+    for other in others:
+        pl.semaphore_signal(barrier, inc=1, device_id={axis: other}, device_id_type=MESH)
+    pl.semaphore_wait(barrier, len(others))
+
+
+def reducer_scratch(rows, width):
+    half = width // 2
+    dma = pltpu.SemaphoreType.DMA
+    return [
+        pltpu.VMEM((3, rows, width), BF16),
+        pltpu.VMEM((rows, width), F32),
+        pltpu.VMEM((rows, half), BF16),
+        pltpu.VMEM((rows, half), BF16),
+        pltpu.VMEM((rows, half), BF16),
+        pltpu.VMEM((rows, half), BF16),
+        pltpu.VMEM((rows, width), BF16),
+        pltpu.VMEM((rows, width), BF16),
+        dma((ROW_PARTS, 6)),
+        dma((ROW_PARTS, 6)),
+    ]
+
+
+def project_kernel(
+    normed_ref, weight_ref, residual_ref, gain_ref, x_ref, after_ref, *scratch
+):
+    buffers, (send, recv, gsend, grecv) = scratch[:8], scratch[8:]
+    red = Reducer("tp", buffers, send, recv)
+    blocks, own = buffers[0], buffers[1]
+    rows, width = own.shape
+    half = width // 2
+    greet("tp", (red.right, red.left))
+
+    def make(owner, slot):
+        source = pl.ds(pl.multiple_of(owner * rows, 64), rows)
+
+        def body(j, carry):
+            columns = pl.ds(pl.multiple_of(j * 256, 256), 256)
+            product = matmul(normed_ref[source, :], weight_ref[:, columns])
+            if slot is None:
+                own[:, columns] = product
+            else:
+                blocks[slot, :, columns] = product.astype(BF16)
+            return carry
+
+        lax.fori_loop(0, width // 256, body, 0)
+
+    make(red.far, 0)
+    red.leg(0, 0).start()
+    red.leg(0, 3).start()
+    make(red.right, 1)
+    red.leg(0, 1).start()
+    make(red.left, 2)
+    red.leg(0, 4).start()
+    make(red.me, None)
+
+    part_rows = red.rows
+
+    def spread(part, index, owner, low, to):
+        where = x_ref.at[
+            pl.ds(pl.multiple_of(owner * rows + part * part_rows, 32), part_rows),
+            pl.ds(low, half),
+        ]
+        return pltpu.make_async_remote_copy(
+            src_ref=where,
+            dst_ref=where,
+            send_sem=gsend.at[part, index],
+            recv_sem=grecv.at[part, index],
+            device_id={"tp": to},
+            device_id_type=MESH,
+        )
+
+    def leaving(part, index):
+        owner = (red.me, red.me, red.left, red.me, red.me, red.right)[index]
+        low = (0, half, 0, half, 0, half)[index]
+        return spread(part, index, owner, low, red.right if index < 3 else red.left)
+
+    def coming(part, index):
+        owner = (red.left, red.left, red.far, red.right, red.right, red.far)[index]
+        low = (0, half, 0, half, 0, half)[index]
+        return spread(part, index, owner, low, red.right if index < 3 else red.left)
+
+    def finish(part):
+        red.wait_final(part)
+
+        def body(i, carry):
+            at = part * part_rows + i * 16
+            here = pl.ds(pl.multiple_of(at, 16), 16)
+            after = (residual_ref[here, :].astype(F32) + red.total(here)).astype(BF16)
+            after_ref[here, :] = after
+            x = after.astype(F32)
+            scale = lax.rsqrt(jnp.mean(x * x, axis=1, keepdims=True) + 1e-06)
+            x_ref[pl.ds(pl.multiple_of(red.me * rows + at, 16), 16), :] = (
+                x * scale * gain_ref[...].astype(F32)
+            ).astype(BF16)
+            return carry
+
+        lax.fori_loop(0, part_rows // 16, body, 0)
+        for n in (0, 3, 1, 4):
+            leaving(part, n).start()
+
+    def pass_on(part):
+        for n in (0, 3):
+            coming(part, n).wait_recv()
+            leaving(part, n + 2).start()
+
+    red.combine(0)
+    for n in (0, 3, 1, 4):
+        red.leg(1, n).start()
+    finish(0)
+    red.combine(1)
+    pass_on(0)
+    finish(1)
+    pass_on(1)
+    for part in range(ROW_PARTS):
+        for n in (1, 2, 4, 5):
+            coming(part, n).wait_recv()
+        for n in range(6):
+            leaving(part, n).wait_send()
+    red.wait_sends()
+
+
+def project(normed, weight, residual, gain):
+    rows, width = residual.shape
+    vmem = pl.BlockSpec(memory_space=pltpu.VMEM)
+    dma = pltpu.SemaphoreType.DMA
+    return pl.pallas_call(
+        project_kernel,
+        out_shape=(
+            jax.ShapeDtypeStruct((4 * rows, width), BF16),
+            jax.ShapeDtypeStruct((rows, width), BF16),
+        ),
+        in_specs=[vmem] * 4,
+        out_specs=(vmem, vmem),
+        scratch_shapes=reducer_scratch(rows, width)
+        + [dma((ROW_PARTS, 6)), dma((ROW_PARTS, 6))],
+        compiler_params=pltpu.CompilerParams(
+            collective_id=2, has_side_effects=True, vmem_limit_bytes=40 * 1024 * 1024
+        ),
+        cost_estimate=pl.CostEstimate(
+            flops=80_000_000_000, bytes_accessed=8_000_000, transcendentals=0
+        ),
+        name="project",
+    )(normed, weight, residual, gain)
+
+
+def feed_kernel(x_ref, stored_ref, after_ref, out_ref, *scratch):
+    buffers, (send, recv, hidden, weight_ref, load_sem) = scratch[:8], scratch[8:]
+    red = Reducer("tp", buffers, send, recv)
+    blocks, own = buffers[0], buffers[1]
+    rows, width = own.shape
+    units = weight_ref.shape[1] // 3
+    tiles = units // 256
+
+    def load(index):
+        if isinstance(index, int) and index == 2 * tiles:
+            columns = pl.ds(2 * units, units)
+        else:
+            columns = pl.ds(pl.multiple_of(index * 256, 256), 256)
+        return pltpu.make_async_copy(
+            stored_ref.at[:, columns], weight_ref.at[:, columns], load_sem.at[index]
+        )
+
+    for j in range(tiles):
+        load(j).start()
+        load(tiles + j).start()
+    load(2 * tiles).start()
+    greet("tp", (red.right, red.left))
+
+    def make(owner, slot, first=False):
+        source = pl.ds(pl.multiple_of(owner * rows, 64), rows)
+
+        def inner(j, carry):
+            low = pl.multiple_of(j * 256, 256)
+            if first:
+                load(j).wait()
+                load(tiles + j).wait()
+            x = x_ref[source, :]
+            gate = matmul(x, weight_ref[:, pl.ds(low, 256)])
+            up = matmul(x, weight_ref[:, pl.ds(pl.multiple_of(units + low, 256), 256)])
+            hidden[:, pl.ds(low, 256)] = (silu_gate(gate) * up).astype(BF16)
+            return carry
+
+        lax.fori_loop(0, tiles, inner, 0)
+        if first:
+            load(2 * tiles).wait()
+
+        def body(j, carry):
+            columns = pl.ds(pl.multiple_of(j * 256, 256), 256)
+            product = matmul(
+                hidden[...], weight_ref[columns, 2 * units : 3 * units], ((1,), (1,))
+            )
+            if slot is None:
+                own[:, columns] = product
+            else:
+                blocks[slot, :, columns] = product.astype(BF16)
+            return carry
+
+        lax.fori_loop(0, width // 256, body, 0)
+
+    make(red.far, 0, True)
+    red.leg(0, 0).start()
+    red.leg(0, 3).start()
+    make(red.right, 1)
+    red.leg(0, 1).start()
+    make(red.left, 2)
+    red.leg(0, 4).start()
+    red.combine(0)
+    for n in (0, 3, 1, 4):
+        red.leg(1, n).start()
+    make(red.me, None)
+
+    def finish(part):
+        red.wait_final(part)
+
+        def body(i, carry):
+            here = pl.ds(pl.multiple_of(part * red.rows + i * 16, 16), 16)
+            out_ref[here, :] = (
+                after_ref[here, :].astype(F32) + 0.5 * red.total(here)
+            ).astype(BF16)
+            return carry
+
+        lax.fori_loop(0, red.rows // 16, body, 0)
+
+    finish(0)
+    red.combine(1)
+    finish(1)
+    red.wait_sends()
+
+
+def feed(x, weight, after):
+    rows, width = after.shape
+    units = weight.shape[1] // 3
+    vmem = pl.BlockSpec(memory_space=pltpu.VMEM)
+    return pl.pallas_call(
+        feed_kernel,
+        out_shape=jax.ShapeDtypeStruct((rows, width), BF16),
+        in_specs=[vmem, pl.BlockSpec(memory_space=pl.ANY), vmem],
+        out_specs=vmem,
+        scratch_shapes=reducer_scratch(rows, width)
+        + [
+            pltpu.VMEM((rows, units), BF16),
+            pltpu.VMEM(weight.shape, BF16),
+            pltpu.SemaphoreType.DMA((2 * units // 256 + 1,)),
+        ],
+        compiler_params=pltpu.CompilerParams(
+            collective_id=3, has_side_effects=True, vmem_limit_bytes=48 * 1024 * 1024
+        ),
+        cost_estimate=pl.CostEstimate(
+            flops=40_000_000_000, bytes_accessed=8_000_000, transcendentals=0
+        ),
+        name="feed",
+    )(x, weight, after)
 
 
 def on_device(
@@ -449,34 +765,12 @@
         ],
         lax.axis_size("sp"),
     )
-    projected = summed_on_arrival(
-        jnp.dot(normed, output_matrix, preferred_element_type=jnp.float32).astype(jnp.bfloat16),
-        "tp",
-        0,
+    x_full, after_mixer = project(
+        normed, output_matrix, residual, feedforward_norm_gain[None]
     )
-    after_mixer = (residual.astype(jnp.float32) + projected).astype(jnp.bfloat16)
-    rows = after_mixer.astype(jnp.float32)
-    x_norm = (
-        rows
-        * lax.rsqrt(jnp.mean(rows * rows, axis=-1, keepdims=True) + 1e-06)
-        * feedforward_norm_gain.astype(jnp.float32)
-    ).astype(jnp.bfloat16)
-    gate_full, up_full, down_full = sent_together((gate_matrix, up_matrix, down_matrix), "sp", 0, 1)
-    x_norm, gate_full, up_full, down_full = lax.optimization_barrier(
-        (x_norm, gate_full, up_full, down_full)
-    )
-    piece = lax.all_gather(x_norm, "tp", axis=0, tiled=True)
-    gate_values = jnp.dot(piece, gate_full, preferred_element_type=jnp.float32)
-    up_values = jnp.dot(piece, up_full, preferred_element_type=jnp.float32)
-    hidden = (jax.nn.silu(gate_values) * up_values).astype(jnp.bfloat16)
-    channel = summed_on_arrival(
-        lax.dot_general(
-            hidden, down_full, (((1,), (1,)), ((), ())), preferred_element_type=jnp.float32
-        ).astype(jnp.bfloat16),
-        "tp",
-        0,
-    )
-    return (after_mixer.astype(jnp.float32) + 0.5 * channel).astype(jnp.bfloat16)
+    shard = jnp.concatenate((gate_matrix, up_matrix, down_matrix), axis=1)
+    weights = lax.all_gather(shard, "sp", axis=0, tiled=True)
+    return feed(x_full, weights, after_mixer)
 
 
 def solution(mesh):

time: 251 us -> 192 us (0.76)
  Pallas kernels: 71.6 us -> 166 us
  waiting for transfers between devices: 79.5 us -> 0.06 us
  blocking collectives: 40.3 us -> 0 us
  matrix products: 22.9 us -> 0 us
  starting transfers between devices: 5.05 us -> 0.01 us
  other arithmetic: 5.48 us -> 1.72 us
    pallas_call x0 -> x2, Pallas kernels: none -> 94.2 us  [the longest x1 56.3 us: project(): pl.pallas_call(project_kernel, out_shape=(jax.ShapeDtypeStruct((4 * rows,...]
    all_gather x2 -> x1, waiting for transfers between devices: 42.2 us -> 0.01 us  [on_device(): weights = lax.all_gather(shard, 'sp', axis=0, tiled=True)]
    all_to_all x1 -> x0, blocking collectives: 40.3 us -> none  [summed_on_arrival(): lax.all_to_all(pieces, axis, split_axis=0, concat_axis=0, tiled=True)]
    all_to_all x1 -> x0, waiting for transfers between devices: 37.2 us -> none  [summed_on_arrival(): lax.all_to_all(pieces, axis, split_axis=0, concat_axis=0, tiled=True)]
    dot_general x3 -> x0, matrix products: 22.9 us -> none  [the longest x1 11.2 us: on_device(): lax.dot_general(hidden, down_full, (((1,), (1,)), ((), ())), preferred_el...]
    split x1 -> x0, local copies, waits for them, and re-layouts: 6.85 us -> none  [sent_together(): jnp.split(lax.all_gather(both, axis, axis=dim, tiled=True), ends, axis=al...]
    all_to_all x1 -> x0, starting transfers between devices: 5.05 us -> none  [summed_on_arrival(): lax.all_to_all(pieces, axis, split_axis=0, concat_axis=0, tiled=True)]
    unnamed x8 -> x13, local copies, waits for them, and re-layouts: 3.97 us -> 7.76 us
  transfers between devices with their start and end apart: 3 -> 1, of which waited for: 2 -> 0; matrix products, arithmetic and copies ran while one was open for 5% -> 3% of each run, Pallas kernels for 29% -> 67%
where the time goes in v1:
time: 192 us; the launch traced here: 191 us
  Pallas kernels  166 us (86%)
  between operations  13.5 us (7%)
  local copies, waits for them, and re-layouts  9.72 us (5%)
    pallas_call x1, Pallas kernels, mixer(): pl.pallas_call(functools.partial(mixer_kernel, peers), out_shape=jax.Shap...  71.5 us
    pallas_call x1, Pallas kernels, project(): pl.pallas_call(project_kernel, out_shape=(jax.ShapeDtypeStruct((4 * rows,...  56.3 us
    pallas_call x1, Pallas kernels, feed(): pl.pallas_call(feed_kernel, out_shape=jax.ShapeDtypeStruct((rows, width),...  37.8 us
    unnamed x13, local copies, waits for them, and re-layouts  7.76 us
  transfers between devices with their start and end apart: 1, of which 0 were waited for; matrix products, arithmetic and copies ran while one was open for 3% of the time, Pallas kernels for 67%

profile of v1, /device:TPU:33, one launch (start us, length us, event | category | flops | bytes accessed | tf_op | source)
XLA Modules:
  0.0 190.7 jit_solution(1712504571357800726)
XLA Ops:
  6.5 0.0 all-gather.2.cloned.1.call-start
  6.6 1.7 pad_maximum_fusion
  8.3 0.1 all-gather.2.cloned.1.call-update
  8.3 1.7 copy.22.step_ref
  10.1 1.7 copy.23.extra_ref
  11.8 1.3 broadcast_in_dim.10.gain_ref
  13.1 0.7 broadcast_in_dim.11.gain_ref
  13.8 0.0 copy-start
  13.8 0.0 copy-start.1
  13.8 71.5 %mixer.1.normed_ref = bf16[768,1024]{1,0:T(8,128)(2,1)} custom-call(bf16[768,1024]{1,0:T(8,128)(2,1)} %value_ref.1, bf16[768,256]{1,0:T(8,128)(2,1)} %wk_ref.1, bf16[768,256]{1,0:T(8,128)(2,1)} %wq_ref.1, bf16[768,128]{1,0:T(8,128)(2,1)} %nk_ref.1, bf16[768,128]{1,0:T(8,128)(2,1)} %nq_ref.1, bf16[768,1024]{1,0:T(8,128)(2,1)} %gate_ref.1, ...), custom_call_target="tpu_custom_call" | custom-call | flops 80000000000 | bytes 8000000 | tf_op jit(solution)/shard_map/mixer/pallas_call | solution.py:351
  85.3 0.0 copy-done
  85.3 0.0 copy-done.1
  85.3 0.0 copy-start.4
  85.3 1.4 copy-done.4
  86.7 56.3 %project.1 = (bf16[768,2048]{1,0:T(8,128)(2,1)S(1)}, bf16[192,2048]{1,0:T(8,128)(2,1)S(1)}) custom-call(bf16[768,1024]{1,0:T(8,128)(2,1)S(1)} %copy-done.4, bf16[1024,2048]{1,0:T(8,128)(2,1)S(1)} %copy-done, bf16[192,2048]{1,0:T(8,128)(2,1)S(1)} %copy-done.1, bf16[1,2048]{1,0:T(2,128)(2,1)S(1)} %broadcast_in_dim.11.gain_ref), custom_call_target="tpu_custom_call" | custom-call | flops 80000000000 | bytes 8000000 | tf_op jit(solution)/shard_map/project/pallas_call | solution.py:596
  143.1 0.0 copy-start.2
  143.1 0.9 copy-done.2
  143.9 0.0 all-gather.2.cloned.1.call-done.stored_ref
  143.9 0.0 copy-start.3
  143.9 1.1 copy-done.3
  145.1 37.8 %feed.1 = bf16[192,2048]{1,0:T(8,128)(2,1)S(1)} custom-call(bf16[768,2048]{1,0:T(8,128)(2,1)S(1)} %get-tuple-element.7.x_ref, bf16[2048,2304]{1,0:T(8,128)(2,1)} %all-gather.2.cloned.1.call-done.stored_ref, bf16[192,2048]{1,0:T(8,128)(2,1)S(1)} %copy-done.3), custom_call_target="tpu_custom_call" | custom-call | flops 40000000000 | bytes 8000000 | tf_op jit(solution)/shard_map/feed/pallas_call | solution.py:704
  182.9 0.9 copy.25
Async XLA Ops:
  6.5 137.4 %all-gather.2.cloned.1.call-start = ((), (), s32[]{:S(2)}) async-start(), calls=%async_computation | async-start | bytes 9732096 | tf_op jit(solution)/shard_map/all_gather | solution.py:772
  13.8 71.5 %copy-start = (bf16[1024,2048]{1,0:T(8,128)(2,1)S(1)}, bf16[1024,2048]{1,0:T(8,128)(2,1)}, u32[]{:S(2)}) copy-start(bf16[1024,2048]{1,0:T(8,128)(2,1)} %weight_ref.1) | copy-start | bytes 12582916
  13.8 71.5 %copy-start.1 = (bf16[192,2048]{1,0:T(8,128)(2,1)S(1)}, bf16[192,2048]{1,0:T(8,128)(2,1)}, u32[]{:S(2)}) copy-start(bf16[192,2048]{1,0:T(8,128)(2,1)} %residual_ref.1) | copy-start | bytes 2359300
  85.3 1.4 copy-start.4
  143.1 0.9 copy-start.2
  143.9 1.1 copy-start.3
Sparse Core Ops, SparseCore 0:
  9.2 114.2 all-gather.1

commit v2 on v1

--- a/solution.py
+++ b/solution.py
@@ -11,6 +11,7 @@
 MESH = pl.DeviceIdType.MESH
 CH = 128
 PAD = 16
+PIECE = 48
 GROUP_Q = (0, 256, 128, 384)
 GROUP_K = (0, 256, 128, 256)
 ROW_GROUP = ((0, 128, 0), (128, 256, 2), (256, 320, 1), (320, 384, 3))
@@ -47,8 +48,9 @@
             return group
 
 
-def mixer_kernel(
+def mixer_part(
     peers,
+    service,
     value_ref,
     wk_ref,
     wq_ref,
@@ -76,18 +78,19 @@
     ebuf,
     hbuf,
     ybuf,
-    out_msg,
-    in_msg,
-    out_ret,
-    in_ret,
     hent,
+    entered_ref,
+    half_out,
+    half_in,
+    chain_in,
+    chain_out,
     local_sem,
     rim_send,
     rim_recv,
-    send_a,
-    recv_a,
-    send_b,
-    recv_b,
+    swap_send,
+    swap_recv,
+    chain_send,
+    chain_recv,
 ):
     length = value_ref.shape[0]
     count = length // CH
@@ -107,30 +110,39 @@
     loads.append(pltpu.make_async_copy(gate_ref, gbuf, local_sem.at[len(inputs)]))
     for load in loads:
         load.start()
-    rims = []
-    if peers > 1:
-        barrier = pltpu.get_barrier_semaphore()
-        for offset in range(1, peers):
-            pl.semaphore_signal(
-                barrier,
-                inc=1,
-                device_id={"sp": lax.rem(me + offset, peers)},
-                device_id_type=MESH,
-            )
-        pl.semaphore_wait(barrier, peers - 1)
-        for n, (ref, (low, high)) in enumerate(zip(inputs, spans)):
-            rims.append(
-                pltpu.make_async_remote_copy(
-                    src_ref=ref.at[pl.ds(length - PAD, PAD)],
-                    dst_ref=xpad.at[pl.ds(0, PAD), pl.ds(low, high - low)],
-                    send_sem=rim_send.at[n],
-                    recv_sem=rim_recv.at[n],
-                    device_id={"sp": lax.rem(me + 1, peers)},
-                    device_id_type=MESH,
-                )
-            )
-        for rim in rims:
-            rim.start()
+    core = lax.rem(me, 2)
+    chip = me // 2
+    chips = peers // 2
+    partner = me + 1 - 2 * core
+
+    def send_to(peer, source, target, send, recv):
+        return pltpu.make_async_remote_copy(
+            src_ref=source,
+            dst_ref=target,
+            send_sem=send,
+            recv_sem=recv,
+            device_id={"sp": peer},
+            device_id_type=MESH,
+        )
+
+    def rim(n):
+        low, high = spans[n]
+        return send_to(
+            lax.rem(me + 1, peers),
+            inputs[n].at[pl.ds(length - PAD, PAD)],
+            xpad.at[pl.ds(0, PAD), pl.ds(low, high - low)],
+            rim_send.at[n],
+            rim_recv.at[n],
+        )
+
+    greet_all(me, peers, service.reply)
+    service.open()
+
+    @pl.when(me < peers - 1)
+    def _():
+        for n in range(len(inputs)):
+            rim(n).start()
+
     for load in loads[:-1]:
         load.wait()
 
@@ -141,6 +153,14 @@
     triu = (row_id <= col_id).astype(F32)
     eye = (row_id == col_id).astype(F32)
     left = lax.broadcasted_iota(jnp.int32, (CH, 128), 1) < 64
+    diagonal = lax.broadcasted_iota(jnp.int32, (16, 16), 0) == lax.broadcasted_iota(
+        jnp.int32, (16, 16), 1
+    )
+    rate = -jnp.sum(
+        jnp.where(diagonal, jnp.broadcast_to(jnp.exp(rate_ref[...]), (16, 16)), 0.0),
+        axis=1,
+        keepdims=True,
+    )
     kernels = (vker_ref, wkker_ref, wqker_ref, nkker_ref, nqker_ref)
 
     def conv_tile(base, which, tile):
@@ -161,20 +181,22 @@
 
         @pl.when(i == count - 1)
         def _():
-            for rim in rims:
-                rim.wait()
+            @pl.when(me > 0)
+            def _():
+                for n in range(len(inputs)):
+                    rim(n).wait_recv()
 
             @pl.when(me == 0)
             def _():
                 xpad[0:PAD, :] = jnp.zeros((PAD, xpad.shape[1]), BF16)
 
         here = pl.ds(base, CH)
-        dt = step_ref[here, :]
-        dt = jnp.maximum(dt, 0.0) + jnp.log(1.0 + jnp.exp(-jnp.abs(dt)))
-        a = -jnp.exp(rate_ref[...]) * dt + extra_ref[here, :]
-        r = matmul(tril, a, precision=HIGH)
-        r_row = matmul(a, triu, ((0,), (0,)), HIGH)
-        dt_row = matmul(dt, eye, ((0,), (0,)), HIGH)
+        dt_row = step_ref[:, here]
+        dt_row = jnp.maximum(dt_row, 0.0) + jnp.log(1.0 + jnp.exp(-jnp.abs(dt_row)))
+        a = rate * dt_row + extra_ref[:, here]
+        r = matmul(tril, a, ((1,), (1,)), HIGH)
+        r_row = matmul(a, triu, precision=HIGH)
+        dt = matmul(eye, dt_row, ((1,), (1,)), HIGH)
         rcol[here, :] = r
         qrow[c] = r_row - jnp.log(dt_row)
         end = r[CH - 1 : CH, :]
@@ -205,6 +227,7 @@
                 ebuf[c, 256:320, :] = e[0:64]
             else:
                 ebuf[c, 320:384, :] = e[64:128]
+        service.run(20 + 14 * i, 34 + 14 * i)
         return carry
 
     lax.fori_loop(0, count, first_pass, 0)
@@ -220,44 +243,23 @@
             state = state * jnp.exp(quad_lanes(total[c], group)) + ebuf[c, low:high, :]
         hent[low:high, :] = state
 
-    if peers > 1:
-        per = 384 // (peers // 2)
-        wide_log = [quad_lanes(whole, group) for group in range(4)]
-        sub = lax.broadcasted_iota(jnp.int32, (8, 128), 0)
-        for slot in range(peers):
-            z, core = slot // 2, slot % 2
-            lanes = slice(128 * core, 128 * core + 128)
-            logs = jnp.zeros((8, 128), F32)
-            for tile in range(per // 8):
-                line = wide_log[group_of_row(per * z + 8 * tile)][:, lanes]
-                logs = jnp.where(sub == tile, jnp.broadcast_to(line, (8, 128)), logs)
-            body = hent[per * z : per * z + per, lanes]
-            out_msg[slot] = jnp.concatenate([body, logs], axis=0).astype(BF16)
-
-        def exchange(source, target, send, recv):
-            order = sorted(range(1, peers), key=lambda o: -min(o, peers - o))
-            copies = []
-            for offset in order:
-                to = lax.rem(me + offset, peers)
-                copies.append(
-                    pltpu.make_async_remote_copy(
-                        src_ref=source.at[to],
-                        dst_ref=target.at[me],
-                        send_sem=send.at[offset],
-                        recv_sem=recv.at[offset],
-                        device_id={"sp": to},
-                        device_id_type=MESH,
-                    )
-                )
-            return copies
-
-        phase_a = exchange(out_msg, in_msg, send_a, recv_a)
-        for copy in phase_a:
-            copy.start()
-        in_msg[me] = out_msg[me]
-
-    for c in range(count):
-        here = slice(c * CH, c * CH + CH)
+    log_total = [quad_lanes(whole, group) for group in range(4)]
+    sub = lax.broadcasted_iota(jnp.int32, (16, 256), 0)
+    swap = send_to(partner, half_out, half_in, swap_send.at[0], swap_recv.at[0])
+
+    @pl.when(core == 0)
+    def _():
+        half_out[0:384, :] = hent[...].astype(BF16)
+        lines = jnp.zeros((16, 256), F32)
+        for group in range(4):
+            lines = jnp.where(
+                sub == group, jnp.broadcast_to(log_total[group], (16, 256)), lines
+            )
+        half_out[384:400, :] = lines.astype(BF16)
+        swap.start()
+
+    def second_pass(c, start):
+        here = pl.ds(pl.multiple_of(c * CH, CH), CH)
         r = rcol[here, :]
         fade_out = jnp.exp(r)
         for group in range(4):
@@ -282,34 +284,81 @@
                 ybuf[here, 128 * pair : 128 * pair + 128] = (
                     inner + outer[:, 128 * half : 128 * half + 128] * pair_lanes(fade_out, 2 * pair)
                 )
-
-    if peers > 1:
-        for copy in phase_a:
-            copy.wait()
-        tiles = per // 8
-        state = [jnp.zeros((8, 128), F32) for _ in range(tiles)]
-        for source in range(peers):
-            out_ret[source] = jnp.concatenate(
-                state + [jnp.zeros((8, 128), F32)], axis=0
-            ).astype(BF16)
-            message = in_msg[source].astype(F32)
-            for tile in range(tiles):
-                decay = jnp.exp(message[per + tile : per + tile + 1, :])
-                state[tile] = state[tile] * decay + message[8 * tile : 8 * tile + 8, :]
-        phase_b = exchange(out_ret, in_ret, send_b, recv_b)
-        for copy in phase_b:
-            copy.start()
-        in_ret[me] = out_ret[me]
-
+        service.run(start + 11 * c, start + 11 * c + 11)
+        return start
+
+    early = jnp.minimum(count, 1 + chip // 2)
+    service.run(20 + 14 * count, 120)
+    lax.fori_loop(0, early, second_pass, 120)
+
+    def link(piece):
+        rows = pl.ds(piece * PIECE, PIECE)
+        return send_to(
+            lax.rem(me + 2, peers),
+            chain_out.at[rows],
+            chain_in.at[rows],
+            chain_send.at[piece],
+            chain_recv.at[piece],
+        )
+
+    hand = send_to(partner, chain_in, entered_ref, swap_send.at[1], swap_recv.at[1])
+
+    @pl.when(core == 1)
+    def _():
+        swap.wait_recv()
+        lines = half_in[384:400, :].astype(F32)
+        fade_0 = [jnp.exp(lines[group : group + 1]) for group in range(4)]
+        fade_1 = [jnp.exp(line) for line in log_total]
+
+        @pl.when(chip == 0)
+        def _():
+            chain_in[...] = jnp.zeros_like(chain_in)
+
+        for piece in range(384 // PIECE):
+
+            @pl.when(chip > 0)
+            def _():
+                link(piece).wait_recv()
+
+            for at in range(piece * PIECE, piece * PIECE + PIECE, 16):
+                group = group_of_row(at)
+                rows = slice(at, at + 16)
+                second = (
+                    chain_in[rows, :].astype(F32) * fade_0[group] + half_in[rows, :].astype(F32)
+                )
+                chain_out[rows, :] = (second * fade_1[group] + hent[rows, :]).astype(BF16)
+                entered_ref[rows, :] = second.astype(BF16)
+
+            @pl.when(chip < chips - 1)
+            def _():
+                link(piece).start()
+
+        hand.start()
+
+    service.run(120 + 11 * early, 130 + 6 * chip)
+    lax.fori_loop(early, count, second_pass, 130 + 6 * chip - 11 * early)
+    at = 130 + 6 * chip + 11 * (count - early)
     loads[-1].wait()
-    if peers > 1:
-        for copy in phase_b:
-            copy.wait()
-        for slot in range(peers):
-            z, core = slot // 2, slot % 2
-            hent[per * z : per * z + per, 128 * core : 128 * core + 128] = in_ret[slot].astype(
-                F32
-            )[:per]
+
+    @pl.when(core == 0)
+    def _():
+        swap.wait_send()
+        hand.wait_recv()
+
+    @pl.when(core == 1)
+    def _():
+        hand.wait_send()
+
+    @pl.when((chip < chips - 1) & (core == 1))
+    def _():
+        for piece in range(384 // PIECE):
+            link(piece).wait_send()
+
+    @pl.when(me < peers - 1)
+    def _():
+        for n in range(len(inputs)):
+            rim(n).wait_send()
+
     ones = (
         (row_id < 64) == (col_id < 64)
     ).astype(BF16)
@@ -318,72 +367,23 @@
         here = slice(c * CH, c * CH + CH)
         reach = jnp.exp(rcol[here, :] + offsets[c])
         for group in range(4):
-            if peers > 1:
-                q = qbuf[here, GROUP_Q[group] : GROUP_Q[group] + 128]
-                row = 0 if group == 0 else 128 if group == 2 else 256
-                entered = matmul(q, hent[row : row + 128, :].astype(BF16))
+            q = qbuf[here, GROUP_Q[group] : GROUP_Q[group] + 128]
+            row = 0 if group == 0 else 128 if group == 2 else 256
+            entered = matmul(q, entered_ref[row : row + 128, :])
             for half in range(2):
                 pair = 2 * group + half
                 lanes = slice(128 * pair, 128 * pair + 128)
                 y = ybuf[here, lanes]
-                if peers > 1:
-                    y = y + entered[:, 128 * half : 128 * half + 128] * pair_lanes(reach, 2 * pair)
+                y = y + entered[:, 128 * half : 128 * half + 128] * pair_lanes(reach, 2 * pair)
                 gated = y * silu(gbuf[here, lanes].astype(F32))
                 square = matmul((gated * gated).astype(BF16), ones)
                 scale = lax.rsqrt(square * (1.0 / 64.0) + 1e-06)
                 normed_ref[here, lanes] = (
                     gated * scale * gain_ref[:, lanes].astype(F32)
                 ).astype(BF16)
-
-
-def mixer(arrays, peers):
-    length = arrays[0].shape[0]
-    width = sum(a.shape[1] for a in arrays[:5])
-    count = length // CH
-    channels = arrays[0].shape[1]
-    message = 384 // max(peers // 2, 1) + 8
-    any_space = pl.BlockSpec(memory_space=pl.ANY)
-    vmem = pl.BlockSpec(memory_space=pltpu.VMEM)
-    dma = pltpu.SemaphoreType.DMA
-    params = dict(vmem_limit_bytes=56 * 1024 * 1024)
-    if peers > 1:
-        params.update(collective_id=1, has_side_effects=True)
-    return pl.pallas_call(
-        functools.partial(mixer_kernel, peers),
-        out_shape=jax.ShapeDtypeStruct((length, channels), BF16),
-        in_specs=[any_space] * 6 + [vmem] * 9,
-        out_specs=vmem,
-        scratch_shapes=[
-            pltpu.VMEM((PAD + length, width), BF16),
-            pltpu.VMEM((length, channels), BF16),
-            pltpu.VMEM((length, 384), BF16),
-            pltpu.VMEM((length, 512), BF16),
-            pltpu.VMEM((length, channels), BF16),
-            pltpu.VMEM((length, 16), F32),
-            pltpu.VMEM((count, 16, CH), F32),
-            pltpu.VMEM((count, 1, 16), F32),
-            pltpu.VMEM((count, 384, 256), F32),
-            pltpu.VMEM((count, 384, 256), BF16),
-            pltpu.VMEM((length, channels), F32),
-            pltpu.VMEM((peers, message, 128), BF16),
-            pltpu.VMEM((peers, message, 128), BF16),
-            pltpu.VMEM((peers, message, 128), BF16),
-            pltpu.VMEM((peers, message, 128), BF16),
-            pltpu.VMEM((384, 256), F32),
-            dma((6,)),
-            dma((5,)),
-            dma((5,)),
-            dma((peers,)),
-            dma((peers,)),
-            dma((peers,)),
-            dma((peers,)),
-        ],
-        compiler_params=pltpu.CompilerParams(**params),
-        cost_estimate=pl.CostEstimate(
-            flops=80_000_000_000, bytes_accessed=8_000_000, transcendentals=0
-        ),
-        name="mixer",
-    )(*arrays)
+        service.run(at, at + 6)
+        at = at + 6
+    return at
 
 
 ROW_PARTS = 2
@@ -464,13 +464,6 @@
             + self.from_l[rows, :].astype(F32)
             + self.from_r[rows, :].astype(F32)
         )
-
-
-def greet(axis, others):
-    barrier = pltpu.get_barrier_semaphore()
-    for other in others:
-        pl.semaphore_signal(barrier, inc=1, device_id={axis: other}, device_id_type=MESH)
-    pl.semaphore_wait(barrier, len(others))
 
 
 def reducer_scratch(rows, width):
@@ -490,15 +483,14 @@
     ]
 
 
-def project_kernel(
-    normed_ref, weight_ref, residual_ref, gain_ref, x_ref, after_ref, *scratch
+def project_part(
+    service, at, normed_ref, weight_ref, residual_ref, gain_ref, x_ref, after_ref, *scratch
 ):
     buffers, (send, recv, gsend, grecv) = scratch[:8], scratch[8:]
     red = Reducer("tp", buffers, send, recv)
     blocks, own = buffers[0], buffers[1]
     rows, width = own.shape
     half = width // 2
-    greet("tp", (red.right, red.left))
 
     def make(owner, slot):
         source = pl.ds(pl.multiple_of(owner * rows, 64), rows)
@@ -517,11 +509,14 @@
     make(red.far, 0)
     red.leg(0, 0).start()
     red.leg(0, 3).start()
+    service.run(at, at + 20)
     make(red.right, 1)
     red.leg(0, 1).start()
     make(red.left, 2)
     red.leg(0, 4).start()
     make(red.me, None)
+    service.open_last()
+    service.run(at + 20, at + 65)
 
     part_rows = red.rows
 
@@ -576,11 +571,17 @@
     red.combine(0)
     for n in (0, 3, 1, 4):
         red.leg(1, n).start()
+    service.run(at + 65, at + 110)
     finish(0)
+    service.run(at + 110, at + 170)
     red.combine(1)
+    service.run(at + 170, at + 270)
     pass_on(0)
+    service.run(at + 270, at + 320)
     finish(1)
+    service.run(at + 320, at + 430)
     pass_on(1)
+    service.close(at + 430)
     for part in range(ROW_PARTS):
         for n in (1, 2, 4, 5):
             coming(part, n).wait_recv()
@@ -589,61 +590,19 @@
     red.wait_sends()
 
 
-def project(normed, weight, residual, gain):
-    rows, width = residual.shape
-    vmem = pl.BlockSpec(memory_space=pltpu.VMEM)
-    dma = pltpu.SemaphoreType.DMA
-    return pl.pallas_call(
-        project_kernel,
-        out_shape=(
-            jax.ShapeDtypeStruct((4 * rows, width), BF16),
-            jax.ShapeDtypeStruct((rows, width), BF16),
-        ),
-        in_specs=[vmem] * 4,
-        out_specs=(vmem, vmem),
-        scratch_shapes=reducer_scratch(rows, width)
-        + [dma((ROW_PARTS, 6)), dma((ROW_PARTS, 6))],
-        compiler_params=pltpu.CompilerParams(
-            collective_id=2, has_side_effects=True, vmem_limit_bytes=40 * 1024 * 1024
-        ),
-        cost_estimate=pl.CostEstimate(
-            flops=80_000_000_000, bytes_accessed=8_000_000, transcendentals=0
-        ),
-        name="project",
-    )(normed, weight, residual, gain)
-
-
-def feed_kernel(x_ref, stored_ref, after_ref, out_ref, *scratch):
-    buffers, (send, recv, hidden, weight_ref, load_sem) = scratch[:8], scratch[8:]
+def feed_part(x_ref, weight_ref, after_ref, out_ref, *scratch):
+    buffers, (send, recv, hidden) = scratch[:8], scratch[8:]
     red = Reducer("tp", buffers, send, recv)
     blocks, own = buffers[0], buffers[1]
     rows, width = own.shape
     units = weight_ref.shape[1] // 3
     tiles = units // 256
 
-    def load(index):
-        if isinstance(index, int) and index == 2 * tiles:
-            columns = pl.ds(2 * units, units)
-        else:
-            columns = pl.ds(pl.multiple_of(index * 256, 256), 256)
-        return pltpu.make_async_copy(
-            stored_ref.at[:, columns], weight_ref.at[:, columns], load_sem.at[index]
-        )
-
-    for j in range(tiles):
-        load(j).start()
-        load(tiles + j).start()
-    load(2 * tiles).start()
-    greet("tp", (red.right, red.left))
-
-    def make(owner, slot, first=False):
+    def make(owner, slot):
         source = pl.ds(pl.multiple_of(owner * rows, 64), rows)
 
         def inner(j, carry):
             low = pl.multiple_of(j * 256, 256)
-            if first:
-                load(j).wait()
-                load(tiles + j).wait()
             x = x_ref[source, :]
             gate = matmul(x, weight_ref[:, pl.ds(low, 256)])
             up = matmul(x, weight_ref[:, pl.ds(pl.multiple_of(units + low, 256), 256)])
@@ -651,8 +610,6 @@
             return carry
 
         lax.fori_loop(0, tiles, inner, 0)
-        if first:
-            load(2 * tiles).wait()
 
         def body(j, carry):
             columns = pl.ds(pl.multiple_of(j * 256, 256), 256)
@@ -667,7 +624,7 @@
 
         lax.fori_loop(0, width // 256, body, 0)
 
-    make(red.far, 0, True)
+    make(red.far, 0)
     red.leg(0, 0).start()
     red.leg(0, 3).start()
     make(red.right, 1)
@@ -697,29 +654,298 @@
     red.wait_sends()
 
 
-def feed(x, weight, after):
-    rows, width = after.shape
-    units = weight.shape[1] // 3
+def greet_all(me, peers, reply):
+    core = lax.rem(me, 2)
+    chip = me // 2
+    last = peers // 2 - 1
+    side = lax.axis_index("tp")
+    barrier = pltpu.get_barrier_semaphore()
+
+    def hail(axis, other):
+        pl.semaphore_signal(barrier, inc=1, device_id={axis: other}, device_id_type=MESH)
+
+    hail("tp", lax.rem(side + 1, 4))
+    hail("tp", lax.rem(side + 3, 4))
+    hail("sp", me + 1 - 2 * core)
+
+    @pl.when(chip > 0)
+    def _():
+        hail("sp", me - 1 - core)
+        hail("sp", me - 2)
+
+    @pl.when(chip < last)
+    def _():
+        hail("sp", me + 2)
+
+    below = (chip > 0).astype(jnp.int32)
+    above = (chip < last).astype(jnp.int32)
+    pl.semaphore_wait(barrier, 3 + below + above + 2 * above * core + 1 - above)
+
+    @pl.when(chip == 0)
+    def _():
+        hail("sp", me + 2 * last)
+
+    @pl.when(chip == last)
+    def _():
+        pl.semaphore_signal(
+            reply, inc=1, device_id={"sp": me - 2 * last}, device_id_type=MESH
+        )
+
+
+class Gatherer:
+    def __init__(self, peers, shards, weights, sems):
+        self.me = lax.axis_index("sp")
+        self.peers = peers
+        self.core = lax.rem(self.me, 2)
+        self.chip = self.me // 2
+        self.chips = peers // 2
+        self.up_steps = self.chips // 2
+        self.down_steps = self.chips - 1 - self.up_steps
+        self.shards, self.weights = shards, weights
+        (self.own_sem, self.up_send, self.up_recv, self.down_send, self.down_recv,
+         self.side_send, self.side_recv, self.reply) = sems
+        self.depth = shards[0].shape[0]
+
+    def own(self, n):
+        units = self.shards[n].shape[1]
+        return pltpu.make_async_copy(
+            self.shards[n],
+            self.weights.at[
+                pl.ds(pl.multiple_of(self.me * self.depth, 64), self.depth), pl.ds(n * units, units)
+            ],
+            self.own_sem.at[n],
+        )
+
+    def begin(self):
+        for n in range(3):
+            self.own(n).start()
+
+    def move(self, chip, core, to, send, recv):
+        place = self.weights.at[
+            pl.ds(pl.multiple_of((2 * chip + core) * self.depth, 64), self.depth)
+        ]
+        return pltpu.make_async_remote_copy(
+            src_ref=place,
+            dst_ref=place,
+            send_sem=send,
+            recv_sem=recv,
+            device_id={"sp": to},
+            device_id_type=MESH,
+        )
+
+    def up(self, k, distance=None):
+        origin = lax.rem(self.chip + self.chips - (k if distance is None else distance), self.chips)
+        to = lax.rem(self.me + 2, self.peers)
+        return self.move(origin, self.core, to, self.up_send.at[k], self.up_recv.at[k])
+
+    def down(self, k, distance=None):
+        origin = lax.rem(self.chip + (k if distance is None else distance), self.chips)
+        to = lax.rem(self.me + self.peers - 2, self.peers)
+        return self.move(origin, self.core, to, self.down_send.at[k], self.down_recv.at[k])
+
+    def side(self, chip, core):
+        to = self.me + 1 - 2 * self.core
+        return self.move(chip, core, to, self.side_send.at[chip], self.side_recv.at[chip])
+
+    def open(self):
+        for n in range(3):
+            self.own(n).wait()
+        self.up(0).start()
+
+        @pl.when(self.chip > 0)
+        def _():
+            self.down(0).start()
+
+        self.side(self.chip, self.core).start()
+
+    def open_last(self):
+        @pl.when(self.chip == 0)
+        def _():
+            pl.semaphore_wait(self.reply, 1)
+            self.down(0).start()
+
+    def due(self, at):
+        near = jnp.maximum((at - 70) // 60, 0)
+        wrapped = (at - 294) // 60
+        up = jnp.minimum(
+            jnp.where(wrapped > self.chip, wrapped, jnp.minimum(near, self.chip)), self.up_steps
+        )
+        near = jnp.maximum((at - 70) // 88, 0)
+        wrapped = (at + 154) // 88
+        down = jnp.minimum(
+            jnp.where(near <= self.chips - 1 - self.chip, near, wrapped), self.down_steps
+        )
+        down = jnp.where((self.chip == 0) & (at < 275), 0, down)
+        return up, down
+
+    def steps(self, first, then):
+        def step_up(i, carry):
+            self.up(i, i + 1).wait_recv()
+
+            @pl.when(i + 1 < self.up_steps)
+            def _():
+                self.up(i + 1).start()
+
+            self.side(lax.rem(self.chip + self.chips - i - 1, self.chips), self.core).start()
+            return carry
+
+        def step_down(i, carry):
+            self.down(i, i + 1).wait_recv()
+
+            @pl.when(i + 1 < self.down_steps)
+            def _():
+                self.down(i + 1).start()
+
+            self.side(lax.rem(self.chip + i + 1, self.chips), self.core).start()
+            return carry
+
+        lax.fori_loop(first[0], then[0], step_up, 0)
+        lax.fori_loop(first[1], then[1], step_down, 0)
+
+    def run(self, at, until):
+        self.steps(self.due(at), self.due(until))
+
+    def close(self, at):
+        self.steps(self.due(at), (self.up_steps, self.down_steps))
+
+        def arrive(i, carry):
+            self.side(i, 1 - self.core).wait_recv()
+            return carry
+
+        lax.fori_loop(0, self.chips, arrive, 0)
+
+    def drain(self):
+        def up(i, carry):
+            self.up(i).wait_send()
+            return carry
+
+        def down(i, carry):
+            self.down(i).wait_send()
+            return carry
+
+        def side(i, carry):
+            self.side(i, self.core).wait_send()
+            return carry
+
+        lax.fori_loop(0, self.up_steps, up, 0)
+        lax.fori_loop(0, self.down_steps, down, 0)
+        lax.fori_loop(0, self.chips, side, 0)
+
+
+def layer_kernel(peers, counts, *refs):
+    refs = list(refs)
+
+    def take(n):
+        out = refs[:n]
+        del refs[:n]
+        return out
+
+    mixer_in = take(15)
+    output_ref, residual_ref, norm_gain_ref = take(3)
+    shards = take(3)
+    (out_ref,) = take(1)
+    (normed,) = take(1)
+    mixer_scratch = take(counts[0])
+    weight, residual, x, after, load_sem = take(5)
+    project_scratch = take(12)
+    feed_scratch = take(11)
+    (weights,) = take(1)
+    sems = take(8)
+    service = Gatherer(peers, shards, weights, sems)
+    service.begin()
+    loads = (
+        pltpu.make_async_copy(output_ref, weight, load_sem.at[0]),
+        pltpu.make_async_copy(residual_ref, residual, load_sem.at[1]),
+    )
+    for load in loads:
+        load.start()
+    at = mixer_part(peers, service, *mixer_in, normed, *mixer_scratch)
+    for load in loads:
+        load.wait()
+    project_part(
+        service, at, normed, weight, residual, norm_gain_ref, x, after, *project_scratch
+    )
+    feed_part(x, weights, after, out_ref, *feed_scratch)
+    service.drain()
+
+
+def layer(arrays, output_matrix, residual, norm_gain, shards, peers):
+    length = arrays[0].shape[0]
+    channels = arrays[0].shape[1]
+    rows, width = residual.shape
+    span = sum(a.shape[1] for a in arrays[:5])
+    depth, units = shards[0].shape
+    count = length // CH
+    hbm = pl.BlockSpec(memory_space=pltpu.HBM)
     vmem = pl.BlockSpec(memory_space=pltpu.VMEM)
+    dma = pltpu.SemaphoreType.DMA
+    chips = peers // 2
+    mixer_scratch = [
+        pltpu.VMEM((PAD + length, span), BF16),
+        pltpu.VMEM((length, channels), BF16),
+        pltpu.VMEM((length, 384), BF16),
+        pltpu.VMEM((length, 512), BF16),
+        pltpu.VMEM((length, channels), BF16),
+        pltpu.VMEM((length, 16), F32),
+        pltpu.VMEM((count, 16, CH), F32),
+        pltpu.VMEM((count, 1, 16), F32),
+        pltpu.VMEM((count, 384, 256), F32),
+        pltpu.VMEM((count, 384, 256), BF16),
+        pltpu.VMEM((length, channels), F32),
+        pltpu.VMEM((384, 256), F32),
+        pltpu.VMEM((384, 256), BF16),
+        pltpu.VMEM((400, 256), BF16),
+        pltpu.VMEM((400, 256), BF16),
+        pltpu.VMEM((384, 256), BF16),
+        pltpu.VMEM((384, 256), BF16),
+        dma((6,)),
+        dma((5,)),
+        dma((5,)),
+        dma((2,)),
+        dma((2,)),
+        dma((384 // PIECE,)),
+        dma((384 // PIECE,)),
+    ]
+    scratch = (
+        [pltpu.VMEM((length, channels), BF16)]
+        + mixer_scratch
+        + [
+            pltpu.VMEM(output_matrix.shape, BF16),
+            pltpu.VMEM((rows, width), BF16),
+            pltpu.VMEM((4 * rows, width), BF16),
+            pltpu.VMEM((rows, width), BF16),
+            dma((2,)),
+        ]
+        + reducer_scratch(rows, width)
+        + [dma((ROW_PARTS, 6)), dma((ROW_PARTS, 6))]
+        + reducer_scratch(rows, width)
+        + [pltpu.VMEM((rows, units), BF16)]
+        + [pltpu.VMEM((peers * depth, 3 * units), BF16)]
+        + [
+            dma((3,)),
+            dma((chips,)),
+            dma((chips,)),
+            dma((chips,)),
+            dma((chips,)),
+            dma((chips,)),
+            dma((chips,)),
+            pltpu.SemaphoreType.REGULAR,
+        ]
+    )
     return pl.pallas_call(
-        feed_kernel,
+        functools.partial(layer_kernel, peers, (len(mixer_scratch),)),
         out_shape=jax.ShapeDtypeStruct((rows, width), BF16),
-        in_specs=[vmem, pl.BlockSpec(memory_space=pl.ANY), vmem],
+        in_specs=[hbm] * 6 + [vmem] * 9 + [hbm, hbm, vmem] + [hbm] * 3,
         out_specs=vmem,
-        scratch_shapes=reducer_scratch(rows, width)
-        + [
-            pltpu.VMEM((rows, units), BF16),
-            pltpu.VMEM(weight.shape, BF16),
-            pltpu.SemaphoreType.DMA((2 * units // 256 + 1,)),
-        ],
+        scratch_shapes=scratch,
         compiler_params=pltpu.CompilerParams(
-            collective_id=3, has_side_effects=True, vmem_limit_bytes=48 * 1024 * 1024
+            collective_id=1, has_side_effects=True, vmem_limit_bytes=62 * 1024 * 1024
         ),
         cost_estimate=pl.CostEstimate(
-            flops=40_000_000_000, bytes_accessed=8_000_000, transcendentals=0
+            flops=40_000_000_000, bytes_accessed=20_000_000, transcendentals=0
         ),
-        name="feed",
-    )(x, weight, after)
+        name="layer",
+    )(*arrays, output_matrix, residual, norm_gain, *shards)
 
 
 def on_device(
@@ -745,7 +971,7 @@
     up_matrix,
     down_matrix,
 ):
-    normed = mixer(
+    return layer(
         [
             value_projected,
             wide_key_rows,
@@ -753,8 +979,8 @@
             narrow_key_rows,
             narrow_query_rows,
             gate_projected,
-            step_before_softplus,
-            extra_log_decay,
+            step_before_softplus.T,
+            extra_log_decay.T,
             log_decay_rate[None],
             value_kernel,
             wide_key_kernel,
@@ -763,14 +989,12 @@
             narrow_query_kernel,
             head_norm_gain[None],
         ],
+        output_matrix,
+        residual,
+        feedforward_norm_gain[None],
+        (gate_matrix, up_matrix, down_matrix),
         lax.axis_size("sp"),
     )
-    x_full, after_mixer = project(
-        normed, output_matrix, residual, feedforward_norm_gain[None]
-    )
-    shard = jnp.concatenate((gate_matrix, up_matrix, down_matrix), axis=1)
-    weights = lax.all_gather(shard, "sp", axis=0, tiled=True)
-    return feed(x_full, weights, after_mixer)
 
 
 def solution(mesh):

time: 192 us -> 165 us (0.86)
  between operations: 13.5 us -> 0.01 us
  Pallas kernels: 166 us -> 160 us
  local copies, waits for them, and re-layouts: 9.72 us -> 4.65 us
    unnamed x13 -> x1, local copies, waits for them, and re-layouts: 7.76 us -> 2.09 us
    pallas_call x3 -> x1, Pallas kernels: 166 us -> 160 us  [layer(): pl.pallas_call(functools.partial(layer_kernel, peers, (len(mixer_scratch)...]
  transfers between devices with their start and end apart: 1 -> 0, of which waited for: 0 -> 0; matrix products, arithmetic and copies ran while one was open for 3% -> 0% of each run, Pallas kernels for 67% -> 0%
where the time goes in v2:
time: 165 us
  Pallas kernels  160 us (97%)
  local copies, waits for them, and re-layouts  4.65 us (3%)
    pallas_call x1, Pallas kernels, layer(): pl.pallas_call(functools.partial(layer_kernel, peers, (len(mixer_scratch)...  160 us

profile of v2, /device:TPU:33, one launch (start us, length us, event | category | flops | bytes accessed | tf_op | source)
XLA Modules:
  0.0 165.0 jit_solution(4891515599348997016)
XLA Ops:
  0.0 1.3 broadcast_in_dim.10.refs_14_
  1.3 1.3 broadcast_in_dim.11.refs_17_
  2.6 160.3 %layer.1 = bf16[192,2048]{1,0:T(8,128)(2,1)} custom-call(bf16[768,1024]{1,0:T(8,128)(2,1)} %refs_0_.1, bf16[768,256]{1,0:T(8,128)(2,1)} %refs_1_.1, bf16[768,256]{1,0:T(8,128)(2,1)} %refs_2_.1, bf16[768,128]{1,0:T(8,128)(2,1)} %refs_3_.1, bf16[768,128]{1,0:T(8,128)(2,1)} %refs_4_.1, bf16[768,1024]{1,0:T(8,128)(2,1)} %refs_5_.1, f32[16,768]{1,0:T(8,128)} %bitcast.3, ...), custom_call_target="tpu_custom_call" | custom-call | flops 40000000000 | bytes 20000000 | tf_op jit(solution)/shard_map/layer/pallas_call | solution.py:935
  162.9 2.1 %copy.23 = bf16[192,2048]{1,0:T(8,128)(2,1)} copy(bf16[192,2048]{1,0:T(8,128)(2,1)} %layer.1) | data formatting | bytes 1572864

commit v3 on v2

--- a/solution.py
+++ b/solution.py
@@ -11,7 +11,7 @@
 MESH = pl.DeviceIdType.MESH
 CH = 128
 PAD = 16
-PIECE = 48
+PIECE = 16
 GROUP_Q = (0, 256, 128, 384)
 GROUP_K = (0, 256, 128, 256)
 ROW_GROUP = ((0, 128, 0), (128, 256, 2), (256, 320, 1), (320, 384, 3))
@@ -509,14 +509,16 @@
     make(red.far, 0)
     red.leg(0, 0).start()
     red.leg(0, 3).start()
-    service.run(at, at + 20)
+    service.run(at, at + 14)
     make(red.right, 1)
     red.leg(0, 1).start()
+    service.run(at + 14, at + 28)
     make(red.left, 2)
     red.leg(0, 4).start()
+    service.run(at + 28, at + 42)
     make(red.me, None)
     service.open_last()
-    service.run(at + 20, at + 65)
+    service.run(at + 42, at + 65)
 
     part_rows = red.rows
 
@@ -692,6 +694,9 @@
         )
 
 
+PARTS = 3
+
+
 class Gatherer:
     def __init__(self, peers, shards, weights, sems):
         self.me = lax.axis_index("sp")
@@ -699,31 +704,30 @@
         self.core = lax.rem(self.me, 2)
         self.chip = self.me // 2
         self.chips = peers // 2
-        self.up_steps = self.chips // 2
-        self.down_steps = self.chips - 1 - self.up_steps
+        self.up_steps = PARTS * (self.chips // 2)
+        self.down_steps = PARTS * (self.chips - 1) - self.up_steps
         self.shards, self.weights = shards, weights
         (self.own_sem, self.up_send, self.up_recv, self.down_send, self.down_recv,
          self.side_send, self.side_recv, self.reply) = sems
         self.depth = shards[0].shape[0]
 
     def own(self, n):
-        units = self.shards[n].shape[1]
         return pltpu.make_async_copy(
-            self.shards[n],
-            self.weights.at[
-                pl.ds(pl.multiple_of(self.me * self.depth, 64), self.depth), pl.ds(n * units, units)
-            ],
-            self.own_sem.at[n],
+            self.shards[n], self.place(self.chip, self.core, n), self.own_sem.at[n]
         )
+
+    def place(self, chip, core, part):
+        units = self.shards[0].shape[1]
+        return self.weights.at[
+            pl.ds(pl.multiple_of((2 * chip + core) * self.depth, 64), self.depth),
+            pl.ds(pl.multiple_of(part * units, 128), units),
+        ]
 
     def begin(self):
         for n in range(3):
             self.own(n).start()
 
-    def move(self, chip, core, to, send, recv):
-        place = self.weights.at[
-            pl.ds(pl.multiple_of((2 * chip + core) * self.depth, 64), self.depth)
-        ]
+    def move(self, place, to, send, recv):
         return pltpu.make_async_remote_copy(
             src_ref=place,
             dst_ref=place,
@@ -733,70 +737,75 @@
             device_id_type=MESH,
         )
 
-    def up(self, k, distance=None):
-        origin = lax.rem(self.chip + self.chips - (k if distance is None else distance), self.chips)
+    def up(self, k, hops=0):
+        distance = k // PARTS + hops
+        origin = lax.rem(self.chip + self.chips - distance, self.chips)
         to = lax.rem(self.me + 2, self.peers)
-        return self.move(origin, self.core, to, self.up_send.at[k], self.up_recv.at[k])
-
-    def down(self, k, distance=None):
-        origin = lax.rem(self.chip + (k if distance is None else distance), self.chips)
+        place = self.place(origin, self.core, lax.rem(k, PARTS))
+        return self.move(place, to, self.up_send.at[k], self.up_recv.at[k])
+
+    def down(self, k, hops=0):
+        distance = k // PARTS + hops
+        origin = lax.rem(self.chip + distance, self.chips)
         to = lax.rem(self.me + self.peers - 2, self.peers)
-        return self.move(origin, self.core, to, self.down_send.at[k], self.down_recv.at[k])
-
-    def side(self, chip, core):
+        place = self.place(origin, self.core, lax.rem(k, PARTS))
+        return self.move(place, to, self.down_send.at[k], self.down_recv.at[k])
+
+    def side(self, k, core):
         to = self.me + 1 - 2 * self.core
-        return self.move(chip, core, to, self.side_send.at[chip], self.side_recv.at[chip])
+        place = self.place(k // PARTS, core, lax.rem(k, PARTS))
+        return self.move(place, to, self.side_send.at[k], self.side_recv.at[k])
 
     def open(self):
-        for n in range(3):
+        for n in range(PARTS):
             self.own(n).wait()
-        self.up(0).start()
-
-        @pl.when(self.chip > 0)
-        def _():
-            self.down(0).start()
-
-        self.side(self.chip, self.core).start()
+            self.up(n).start()
+
+            @pl.when(self.chip > 0)
+            def _():
+                self.down(n).start()
+
+            self.side(self.chip * PARTS + n, self.core).start()
 
     def open_last(self):
         @pl.when(self.chip == 0)
         def _():
             pl.semaphore_wait(self.reply, 1)
-            self.down(0).start()
+            for n in range(PARTS):
+                self.down(n).start()
 
     def due(self, at):
-        near = jnp.maximum((at - 70) // 60, 0)
-        wrapped = (at - 294) // 60
+        near = jnp.maximum((at - 55) // 20, 0)
+        wrapped = (at - 279) // 20
+        limit = PARTS * self.chip
         up = jnp.minimum(
-            jnp.where(wrapped > self.chip, wrapped, jnp.minimum(near, self.chip)), self.up_steps
+            jnp.where(wrapped > limit, wrapped, jnp.minimum(near, limit)), self.up_steps
         )
-        near = jnp.maximum((at - 70) // 88, 0)
-        wrapped = (at + 154) // 88
-        down = jnp.minimum(
-            jnp.where(near <= self.chips - 1 - self.chip, near, wrapped), self.down_steps
-        )
+        down = jnp.minimum(jnp.maximum((at - 90) // 27, 0), self.down_steps)
         down = jnp.where((self.chip == 0) & (at < 275), 0, down)
         return up, down
 
     def steps(self, first, then):
         def step_up(i, carry):
-            self.up(i, i + 1).wait_recv()
-
-            @pl.when(i + 1 < self.up_steps)
+            self.up(i, 1).wait_recv()
+
+            @pl.when(i + PARTS < self.up_steps)
             def _():
-                self.up(i + 1).start()
-
-            self.side(lax.rem(self.chip + self.chips - i - 1, self.chips), self.core).start()
+                self.up(i + PARTS).start()
+
+            origin = lax.rem(self.chip + self.chips - i // PARTS - 1, self.chips)
+            self.side(origin * PARTS + lax.rem(i, PARTS), self.core).start()
             return carry
 
         def step_down(i, carry):
-            self.down(i, i + 1).wait_recv()
-
-            @pl.when(i + 1 < self.down_steps)
+            self.down(i, 1).wait_recv()
+
+            @pl.when(i + PARTS < self.down_steps)
             def _():
-                self.down(i + 1).start()
-
-            self.side(lax.rem(self.chip + i + 1, self.chips), self.core).start()
+                self.down(i + PARTS).start()
+
+            origin = lax.rem(self.chip + i // PARTS + 1, self.chips)
+            self.side(origin * PARTS + lax.rem(i, PARTS), self.core).start()
             return carry
 
         lax.fori_loop(first[0], then[0], step_up, 0)
@@ -812,7 +821,7 @@
             self.side(i, 1 - self.core).wait_recv()
             return carry
 
-        lax.fori_loop(0, self.chips, arrive, 0)
+        lax.fori_loop(0, PARTS * self.chips, arrive, 0)
 
     def drain(self):
         def up(i, carry):
@@ -829,7 +838,7 @@
 
         lax.fori_loop(0, self.up_steps, up, 0)
         lax.fori_loop(0, self.down_steps, down, 0)
-        lax.fori_loop(0, self.chips, side, 0)
+        lax.fori_loop(0, PARTS * self.chips, side, 0)
 
 
 def layer_kernel(peers, counts, *refs):
@@ -923,12 +932,12 @@
         + [pltpu.VMEM((peers * depth, 3 * units), BF16)]
         + [
             dma((3,)),
-            dma((chips,)),
-            dma((chips,)),
-            dma((chips,)),
-            dma((chips,)),
-            dma((chips,)),
-            dma((chips,)),
+            dma((PARTS * chips,)),
+            dma((PARTS * chips,)),
+            dma((PARTS * chips,)),
+            dma((PARTS * chips,)),
+            dma((PARTS * chips,)),
+            dma((PARTS * chips,)),
             pltpu.SemaphoreType.REGULAR,
         ]
     )

time: 165 us -> 149 us (0.903)
  Pallas kernels: 160 us -> 144 us
    pallas_call x1, Pallas kernels: 160 us -> 144 us  [layer(): pl.pallas_call(functools.partial(layer_kernel, peers, (len(mixer_scratch)...]
where the time goes in v3:
time: 149 us
  Pallas kernels  144 us (97%)
  local copies, waits for them, and re-layouts  4.65 us (3%)
    pallas_call x1, Pallas kernels, layer(): pl.pallas_call(functools.partial(layer_kernel, peers, (len(mixer_scratch)...  144 us

profile of v3, /device:TPU:33, one launch (start us, length us, event | category | flops | bytes accessed | tf_op | source)
XLA Modules:
  0.0 149.0 jit_solution(13545977020655494192)
XLA Ops:
  0.0 1.3 broadcast_in_dim.10.refs_14_
  1.3 1.3 broadcast_in_dim.11.refs_17_
  2.6 144.4 %layer.1 = bf16[192,2048]{1,0:T(8,128)(2,1)} custom-call(bf16[768,1024]{1,0:T(8,128)(2,1)} %refs_0_.1, bf16[768,256]{1,0:T(8,128)(2,1)} %refs_1_.1, bf16[768,256]{1,0:T(8,128)(2,1)} %refs_2_.1, bf16[768,128]{1,0:T(8,128)(2,1)} %refs_3_.1, bf16[768,128]{1,0:T(8,128)(2,1)} %refs_4_.1, bf16[768,1024]{1,0:T(8,128)(2,1)} %refs_5_.1, f32[16,768]{1,0:T(8,128)} %bitcast.3, ...), custom_call_target="tpu_custom_call" | custom-call | flops 40000000000 | bytes 20000000 | tf_op jit(solution)/shard_map/layer/pallas_call | solution.py:944
  147.0 2.1 %copy.23 = bf16[192,2048]{1,0:T(8,128)(2,1)} copy(bf16[192,2048]{1,0:T(8,128)(2,1)} %layer.1) | data formatting | bytes 1572864

commit v4 on v3

--- a/solution.py
+++ b/solution.py
@@ -84,6 +84,9 @@
     half_in,
     chain_in,
     chain_out,
+    pair_out,
+    pair_in,
+    give,
     local_sem,
     rim_send,
     rim_recv,
@@ -287,21 +290,26 @@
         service.run(start + 11 * c, start + 11 * c + 11)
         return start
 
-    early = jnp.minimum(count, 1 + chip // 2)
+    early = jnp.where(chip == 0, 1, count)
     service.run(20 + 14 * count, 120)
     lax.fori_loop(0, early, second_pass, 120)
-
-    def link(piece):
+    odd = lax.rem(chip, 2)
+    sends_on = (chip < chips - 1) & (core * odd == 1)
+
+    def link(piece, hops):
         rows = pl.ds(piece * PIECE, PIECE)
         return send_to(
-            lax.rem(me + 2, peers),
+            lax.rem(me + 2 * hops, peers),
             chain_out.at[rows],
             chain_in.at[rows],
-            chain_send.at[piece],
+            chain_send.at[hops - 1, piece],
             chain_recv.at[piece],
         )
 
-    hand = send_to(partner, chain_in, entered_ref, swap_send.at[1], swap_recv.at[1])
+    hand = send_to(partner, give, entered_ref, swap_send.at[1], swap_recv.at[1])
+    couple = send_to(
+        lax.rem(me + 2, peers), pair_out, pair_in, swap_send.at[2], swap_recv.at[2]
+    )
 
     @pl.when(core == 1)
     def _():
@@ -310,34 +318,63 @@
         fade_0 = [jnp.exp(lines[group : group + 1]) for group in range(4)]
         fade_1 = [jnp.exp(line) for line in log_total]
 
-        @pl.when(chip == 0)
+        @pl.when(odd == 0)
+        def _():
+            for at in range(0, 384, 16):
+                rows = slice(at, at + 16)
+                pair_out[rows, :] = (
+                    half_in[rows, :].astype(F32) * fade_1[group_of_row(at)] + hent[rows, :]
+                ).astype(BF16)
+            both = jnp.zeros((16, 256), F32)
+            for group in range(4):
+                line = lines[group : group + 1] + log_total[group]
+                both = jnp.where(sub == group, jnp.broadcast_to(line, (16, 256)), both)
+            pair_out[384:400, :] = both.astype(BF16)
+            couple.start()
+
+        @pl.when(odd == 1)
+        def _():
+            couple.wait_recv()
+
+        @pl.when(odd == 0)
+        def _():
+            pair_in[...] = jnp.zeros_like(pair_in)
+
+        @pl.when(chip < 2)
         def _():
             chain_in[...] = jnp.zeros_like(chain_in)
 
+        pair_lines = pair_in[384:400, :].astype(F32)
+        fade_pair = [jnp.exp(pair_lines[group : group + 1]) for group in range(4)]
+
         for piece in range(384 // PIECE):
 
-            @pl.when(chip > 0)
+            @pl.when(chip > 1)
             def _():
-                link(piece).wait_recv()
+                link(piece, 1).wait_recv()
 
             for at in range(piece * PIECE, piece * PIECE + PIECE, 16):
                 group = group_of_row(at)
                 rows = slice(at, at + 16)
-                second = (
-                    chain_in[rows, :].astype(F32) * fade_0[group] + half_in[rows, :].astype(F32)
+                prior = (
+                    chain_in[rows, :].astype(F32) * fade_pair[group]
+                    + pair_in[rows, :].astype(F32)
                 )
+                second = prior * fade_0[group] + half_in[rows, :].astype(F32)
                 chain_out[rows, :] = (second * fade_1[group] + hent[rows, :]).astype(BF16)
                 entered_ref[rows, :] = second.astype(BF16)
-
-            @pl.when(chip < chips - 1)
+                give[rows, :] = prior.astype(BF16)
+
+            @pl.when(sends_on)
             def _():
-                link(piece).start()
+                link(piece, 2).start()
+                link(piece, 1).start()
 
         hand.start()
 
-    service.run(120 + 11 * early, 130 + 6 * chip)
-    lax.fori_loop(early, count, second_pass, 130 + 6 * chip - 11 * early)
-    at = 130 + 6 * chip + 11 * (count - early)
+    service.run(120 + 11 * early, 130 + 11 * early)
+    lax.fori_loop(early, count, second_pass, 130)
+    at = 130 + 11 * count
     loads[-1].wait()
 
     @pl.when(core == 0)
@@ -349,10 +386,15 @@
     def _():
         hand.wait_send()
 
-    @pl.when((chip < chips - 1) & (core == 1))
+        @pl.when(odd == 0)
+        def _():
+            couple.wait_send()
+
+    @pl.when(sends_on)
     def _():
         for piece in range(384 // PIECE):
-            link(piece).wait_send()
+            link(piece, 1).wait_send()
+            link(piece, 2).wait_send()
 
     @pl.when(me < peers - 1)
     def _():
@@ -379,7 +421,7 @@
                 square = matmul((gated * gated).astype(BF16), ones)
                 scale = lax.rsqrt(square * (1.0 / 64.0) + 1e-06)
                 normed_ref[here, lanes] = (
-                    gated * scale * gain_ref[:, lanes].astype(F32)
+                    gated * scale * gain_ref[pair : pair + 1, :].astype(F32)
                 ).astype(BF16)
         service.run(at, at + 6)
         at = at + 6
@@ -546,6 +588,9 @@
         low = (0, half, 0, half, 0, half)[index]
         return spread(part, index, owner, low, red.right if index < 3 else red.left)
 
+    gain = gain_ref[...].astype(F32)
+    gain = jnp.concatenate([gain[n : n + 1] for n in range(width // 128)], axis=1)
+
     def finish(part):
         red.wait_final(part)
 
@@ -557,7 +602,7 @@
             x = after.astype(F32)
             scale = lax.rsqrt(jnp.mean(x * x, axis=1, keepdims=True) + 1e-06)
             x_ref[pl.ds(pl.multiple_of(red.me * rows + at, 16), 16), :] = (
-                x * scale * gain_ref[...].astype(F32)
+                x * scale * gain
             ).astype(BF16)
             return carry
 
@@ -681,7 +726,14 @@
 
     below = (chip > 0).astype(jnp.int32)
     above = (chip < last).astype(jnp.int32)
-    pl.semaphore_wait(barrier, 3 + below + above + 2 * above * core + 1 - above)
+    odd = lax.rem(chip, 2)
+
+    @pl.when((chip > 1) & (core * odd == 1))
+    def _():
+        hail("sp", me - 4)
+
+    far = above * core * odd
+    pl.semaphore_wait(barrier, 3 + below + above + 2 * above * core + 1 - above + far)
 
     @pl.when(chip == 0)
     def _():
@@ -704,7 +756,7 @@
         self.core = lax.rem(self.me, 2)
         self.chip = self.me // 2
         self.chips = peers // 2
-        self.up_steps = PARTS * (self.chips // 2)
+        self.up_steps = PARTS * (self.chips // 2 - 1)
         self.down_steps = PARTS * (self.chips - 1) - self.up_steps
         self.shards, self.weights = shards, weights
         (self.own_sem, self.up_send, self.up_recv, self.down_send, self.down_recv,
@@ -907,12 +959,15 @@
         pltpu.VMEM((400, 256), BF16),
         pltpu.VMEM((384, 256), BF16),
         pltpu.VMEM((384, 256), BF16),
+        pltpu.VMEM((400, 256), BF16),
+        pltpu.VMEM((400, 256), BF16),
+        pltpu.VMEM((384, 256), BF16),
         dma((6,)),
         dma((5,)),
         dma((5,)),
-        dma((2,)),
-        dma((2,)),
-        dma((384 // PIECE,)),
+        dma((3,)),
+        dma((3,)),
+        dma((2, 384 // PIECE)),
         dma((384 // PIECE,)),
     ]
     scratch = (
@@ -996,11 +1051,11 @@
             wide_query_kernel,
             narrow_key_kernel,
             narrow_query_kernel,
-            head_norm_gain[None],
+            head_norm_gain.reshape(-1, 128),
         ],
         output_matrix,
         residual,
-        feedforward_norm_gain[None],
+        feedforward_norm_gain.reshape(-1, 128),
         (gate_matrix, up_matrix, down_matrix),
         lax.axis_size("sp"),
     )

time: 149 us -> 148 us (level)
  the two profiles are of different devices: /device:TPU:33 before, /device:TPU:421 now
where the time goes in v4:
time: 148 us; the launch traced here: 147 us
  Pallas kernels  145 us (98%)
  local copies, waits for them, and re-layouts  2.09 us (1%)
    pallas_call x1, Pallas kernels, layer(): pl.pallas_call(functools.partial(layer_kernel, peers, (len(mixer_scratch)...  145 us

profile of v4, /device:TPU:421, one launch (start us, length us, event | category | flops | bytes accessed | tf_op | source)
XLA Modules:
  0.0 147.5 jit_solution(16683184323088609386)
XLA Ops:
  0.0 145.4 %layer.1 = bf16[192,2048]{1,0:T(8,128)(2,1)} custom-call(bf16[768,1024]{1,0:T(8,128)(2,1)} %refs_0_.1, bf16[768,256]{1,0:T(8,128)(2,1)} %refs_1_.1, bf16[768,256]{1,0:T(8,128)(2,1)} %refs_2_.1, bf16[768,128]{1,0:T(8,128)(2,1)} %refs_3_.1, bf16[768,128]{1,0:T(8,128)(2,1)} %refs_4_.1, bf16[768,1024]{1,0:T(8,128)(2,1)} %refs_5_.1, f32[16,768]{1,0:T(8,128)} %bitcast.5, ...), custom_call_target="tpu_custom_call" | custom-call | flops 40000000000 | bytes 20000000 | tf_op jit(solution)/shard_map/layer/pallas_call | solution.py:999
  145.4 2.1 %copy.23 = bf16[192,2048]{1,0:T(8,128)(2,1)} copy(bf16[192,2048]{1,0:T(8,128)(2,1)} %layer.1) | data formatting | bytes 1572864
